TPU v7x, 128 devices: a whole 4x4x4 slice. The times are simulated.
128 devices in a mesh: fs: 16 (over z, x), tp: 8 (over y, core).
Axes of the slice: x: 4, y: 4, z: 4, core: 2. Of those that a mesh axis runs over, the one named last changes fastest.
Arguments:
- layer_inputs: bfloat16 [40960, 2048], P('fs'), may hold values from -6 to 6
- output_cot: bfloat16 [40960, 2048], P('fs'), may hold values from -6 to 6
- query_cot: bfloat16 [40960, 2048], P('fs', 'tp'), may hold values from -6 to 6
- head_outputs: bfloat16 [40960, 2048], P('fs', 'tp'), may hold values from -6 to 6
- weights: float32 [2, 2048, 2048], P(None, 'fs', 'tp'), may hold values from -0.125 to 0.125
- factors: bfloat16 [2, 2048, 256], replicated, may hold values from -0.125 to 0.125
- first_moment: float32 [2, 256, 2048], P(None, None, 'tp'), may hold values from -600 to 600
- second_moment: float32 [2, 256, 2048], P(None, None, 'tp'), may hold values from 1000 to 100000
Outputs:
- new_weights: float32 [2, 2048, 2048], P(None, 'fs', 'tp')
- update: float32 [2, 2048, 2048], P(None, 'fs', 'tp')
- new_first: float32 [2, 256, 2048], P(None, None, 'tp')
- new_second: float32 [2, 256, 2048], P(None, None, 'tp')
- weight_copy: bfloat16 [2, 2048, 2048], P(None, None, 'tp')
All inputs are finite; a program needn't handle non-finite values.
Results may differ from a plain program's by a relative error of at most 0.00055.
Values may be sent and summed in bfloat16 or wider, within the bound.
A program may use at most 128 MiB of HBM per device.

v0:
```python
from functools import partial

import jax
import jax.numpy as jnp
from jax import lax
from jax.sharding import Mesh
from jax.sharding import PartitionSpec as P

D = 2048
QDIM = 2048
FS = ("fs_0", "fs_1")
TP = ("tp_0", "tp_1")
FS_TP = ("fs_0", "fs_1", "tp_0", "tp_1")


def in_blocks(array, dim, length):
    shape = array.shape
    pieces = array.reshape(*shape[:dim], length, shape[dim] // length, *shape[dim + 1 :])
    return jnp.moveaxis(pieces, dim, 0)


def summed_on_arrival(array, axis, dim):
    pieces = in_blocks(array, dim, lax.axis_size(axis))
    arrived = lax.all_to_all(pieces, axis, split_axis=0, concat_axis=0, tiled=True)
    return arrived.sum(axis=0)


def sent_to_all(array, axis):
    copies = jnp.broadcast_to(array, (lax.axis_size(axis), *array.shape))
    return lax.all_to_all(copies, axis, split_axis=0, concat_axis=0, tiled=True)


def laid_out(pieces, dim):
    shape = list(pieces.shape[1:])
    shape[dim] *= pieces.shape[0]
    return jnp.moveaxis(pieces, 0, dim).reshape(shape)


def collect(array, axis, dim):
    pieces = sent_to_all(array, axis)
    return laid_out(pieces, dim)


def taken_together(array, axis):
    return sent_to_all(array, axis).sum(axis=0)


def by_axis(array, axes):
    for axis in axes:
        array = lax.psum(array, axis)
    return array


def block_terms(lefts, rights, projected, row_dev, extra, block, start, count):
    blocks = count // block
    first_block = start // block
    pieces = []
    for index in range(len(lefts)):
        columns = lefts[index]
        grad = lax.dot_general(
            columns, rights[index], (((0,), (0,)), ((), ())), preferred_element_type=jnp.float32
        )
        pieces.append(grad.reshape(blocks, row_dev, -1))
        lowcols = projected[index]
        high_part = lowcols.astype(jnp.bfloat16)
        restored = lax.optimization_barrier(high_part).astype(jnp.float32)
        low_part = (lowcols - restored).astype(jnp.bfloat16)
        part = lax.dot_general(
            high_part, rights[index], (((0,), (0,)), ((), ())), preferred_element_type=jnp.float32
        )
        part = part + lax.dot_general(
            low_part, rights[index], (((0,), (0,)), ((), ())), preferred_element_type=jnp.float32
        )
        pieces.append(part.reshape(blocks, extra, -1))
    return jnp.concatenate(pieces, axis=1).reshape(count, -1)


def per_device(
    layer_inputs, output_cot, query_cot, head_outputs, weights, factors, first_moment, second_moment
):
    lefts = (layer_inputs, output_cot)
    rights = (query_cot, head_outputs)
    row_dev = weights.shape[1]
    fs_count = lax.axis_size(FS)
    position = lax.axis_index(FS)
    projected = tuple(
        (
            jnp.dot(lefts[index], factors[index], preferred_element_type=jnp.float32)
            for index in range(2)
        )
    )
    extra = factors.shape[2] // fs_count
    block = 2 * (row_dev + extra)
    both = partial(block_terms, lefts, rights, projected, row_dev, extra, block)
    rows_all = summed_on_arrival(both(jnp.int32(0), block * lax.axis_size(FS)), FS, 0).reshape(
        2, row_dev + extra, -1
    )
    grads = rows_all[:, :row_dev]
    own_factors = lax.dynamic_slice_in_dim(factors, position * row_dev, row_dev, 1).astype(
        jnp.float32
    )
    low = collect(rows_all[:, row_dev:], FS, 1)
    first = 0.9 * first_moment + 0.1 * low
    second = 0.95 * second_moment + 0.05 * low * low
    normed = first / (jnp.sqrt(second) + 1e-06)
    sums = taken_together(
        jnp.stack([jnp.sum(normed * normed, axis=(1, 2)), jnp.sum(low * low, axis=(1, 2))]), TP
    )
    ratio = jnp.sqrt(sums[0]) / jnp.sqrt(sums[1] + 1e-06)
    resid = grads - jnp.einsum("kdr,krq->kdq", own_factors, low, precision=lax.Precision.HIGHEST)
    step = (
        jnp.einsum("kdr,krq->kdq", own_factors, normed, precision=lax.Precision.HIGHEST)
        + ratio[:, None, None] * resid
    )
    total = by_axis(jnp.sum(step * step), FS_TP)
    update = step * lax.rsqrt(total / (2.0 * D * QDIM) + 1e-06)
    new_weights = weights - 0.02 * update
    weight_copy = collect(new_weights.astype(jnp.bfloat16), FS, 1)
    return (new_weights, update, first, second, weight_copy)


def solution(mesh):
    finer = Mesh(mesh.devices.reshape(4, 4, 4, 2), ("fs_0", "fs_1", "tp_0", "tp_1"))
    in_specs = (
        P(FS, None),
        P(FS, None),
        P(FS, TP),
        P(FS, TP),
        P(None, FS, TP),
        P(),
        P(None, None, TP),
        P(None, None, TP),
    )
    out_specs = (
        P(None, FS, TP),
        P(None, FS, TP),
        P(None, None, TP),
        P(None, None, TP),
        P(None, None, TP),
    )
    return jax.shard_map(
        per_device, mesh=finer, in_specs=in_specs, out_specs=out_specs, check_vma=False
    )
```

profile of v0, /device:TPU:0, one launch (start us, length us, event | category | flops | bytes accessed | tf_op | source)
XLA Modules:
  0.0 186.5 jit_solution(15196793346113739314)
XLA Ops:
  0.6 0.0 copy-start
  0.7 6.1 %fusion.17 = (bf16[2560,256]{1,0:T(8,128)(2,1)S(1)}, f32[2560,256]{1,0:T(8,128)S(1)}) fusion(bf16[2560,2048]{1,0:T(8,128)(2,1)} %param.8, bf16[2,2048,256]{2,1,0:T(8,128)(2,1)} %param.13), kind=kOutput, calls=%fused_computation.33 | convolution fusion | flops 2685009920 | bytes 15466496 | tf_op jit(solution)/shard_map/dot_general | solution.py:88
  6.8 1.6 copy-done.5
  8.4 3.4 %fusion.18 = f32[2048,256]{1,0:T(8,128)S(1)} fusion(bf16[2560,2048]{1,0:T(8,128)(2,1)S(1)} %copy-done.5, bf16[2560,256]{1,0:T(8,128)(2,1)S(1)} %copy-done), kind=kOutput, calls=%fused_computation.34 | convolution fusion | flops 2684354560 | bytes 13893632 | tf_op jit(solution)/shard_map/dot_general | solution.py:60
  11.8 0.6 fusion
  12.4 0.5 convolution_add_fusion.2
  13.0 1.0 copy-done.4
  14.0 3.1 %fusion.16 = (bf16[2560,256]{1,0:T(8,128)(2,1)S(1)}, f32[2560,256]{1,0:T(8,128)S(1)}) fusion(bf16[2560,2048]{1,0:T(8,128)(2,1)S(1)} %bitcast.54, bf16[2,2048,256]{2,1,0:T(8,128)(2,1)S(1)} %copy-done.4), kind=kOutput, calls=%fused_computation.32 | convolution fusion | flops 2685009920 | bytes 15466496 | tf_op jit(solution)/shard_map/dot_general | solution.py:88
  17.1 3.3 %fusion.19 = f32[2048,256]{1,0:T(8,128)S(1)} fusion(bf16[2560,2048]{1,0:T(8,128)(2,1)S(1)} %bitcast.54, bf16[2560,256]{1,0:T(8,128)(2,1)S(1)} %copy-done.1), kind=kOutput, calls=%fused_computation.35 | convolution fusion | flops 2684354560 | bytes 13893632 | tf_op jit(solution)/shard_map/dot_general | solution.py:60
  20.4 0.6 fusion.1
  21.0 0.5 convolution_add_fusion.1
  21.5 0.4 pad_maximum_fusion
  22.0 64.4 %all_to_all.20 = f32[16,288,256]{2,1,0:T(8,128)} all-to-all(f32[16,288,256]{2,1,0:T(8,128)S(1)} %pad_maximum_fusion), channel_id=1, replica_groups=mesh['fs_0'=4,'fs_1'=4,'tp_0'=4,'tp_1'=2] {'fs_0','fs_1'}, dimensions={0} | all-to-all | bytes 9437184 | tf_op jit(solution)/shard_map/all_to_all | solution.py:24
  86.4 2.7 %reduce_sum.45 = f32[288,256]{1,0:T(8,128)S(1)} reduce(f32[16,288,256]{2,1,0:T(8,128)} %all_to_all.20, f32[]{:T(128)} %constant.9.clone.1), dimensions={0}, to_apply=%region_0.0 | reduce | flops 1105920 | bytes 5013508 | tf_op jit(solution)/shard_map/reduce_sum | solution.py:25
  89.1 0.9 broadcast_in_dim.10
  89.9 3.6 %all-to-all-start.1 = ((f32[16,2,16,256]{3,2,1,0:T(8,128)}), f32[16,2,16,256]{3,2,1,0:T(8,128)S(1)}, u32[]{:S(2)}, u32[]{:S(2)}) async-start(f32[16,2,16,256]{3,2,1,0:T(8,128)} %broadcast_in_dim.10), calls=%async_computation.1 | async-start | bytes 1048576 | tf_op jit(solution)/shard_map/all_to_all | solution.py:30
  93.5 10.4 %all-to-all-done.1 = f32[16,2,16,256]{3,2,1,0:T(8,128)S(1)} async-done(((f32[16,2,16,256]{3,2,1,0:T(8,128)}), f32[16,2,16,256]{3,2,1,0:T(8,128)S(1)}, u32[]{:S(2)}, u32[]{:S(2)}) %all-to-all-start.1) | async-done | bytes 524320 | tf_op jit(solution)/shard_map/all_to_all | solution.py:30
  104.0 2.4 %multiply_reduce_fusion.1 = (f32[2]{0:T(128)S(1)}, f32[2,256,256]{2,1,0:T(8,128)}, f32[2,256,256]{2,1,0:T(8,128)}) fusion(f32[2,16,16,256]{3,2,1,0:T(8,128)S(1)} %copy.18, f32[2,256,256]{2,1,0:T(8,128)S(1)} %copy-done.2, f32[2,256,256]{2,1,0:T(8,128)} %param.14), kind=kLoop, calls=%fused_computation.19 | loop fusion | flops 1441790 | bytes 2621448 | tf_op jit(solution)/shard_map/reduce_sum | solution.py:107
  106.3 0.2 multiply_reduce_fusion
  106.5 0.6 broadcast_in_dim.11
  107.1 4.5 %all-to-all-start.2 = ((f32[8,2,2]{2,1,0:T(2,128)}), f32[8,2,2]{2,1,0:T(2,128)S(1)}, u32[]{:S(2)}, u32[]{:S(2)}) async-start(f32[8,2,2]{2,1,0:T(2,128)} %broadcast_in_dim.11), calls=%async_computation.2 | async-start | bytes 16384 | tf_op jit(solution)/shard_map/all_to_all | solution.py:30
  111.6 5.3 %all-to-all-done.2 = f32[8,2,2]{2,1,0:T(2,128)S(1)} async-done(((f32[8,2,2]{2,1,0:T(2,128)}), f32[8,2,2]{2,1,0:T(2,128)S(1)}, u32[]{:S(2)}, u32[]{:S(2)}) %all-to-all-start.2) | async-done | bytes 160 | tf_op jit(solution)/shard_map/all_to_all | solution.py:30
  116.9 1.3 fusion.2
  118.2 2.4 %multiply_reduce_fusion.2 = (f32[]{:T(128)}, f32[2,128,256]{2,1,0:T(8,128)S(1)}) fusion(f32[2,128,256]{2,1,0:T(8,128)S(1)} %fusion.2, f32[2,256,256]{2,1,0:T(8,128)} %get-tuple-element.10, f32[2,256,256]{2,1,0:T(8,128)} %get-tuple-element.9, bf16[2,2048,256]{2,1,0:T(8,128)(2,1)} %param.13, s32[]{:T(128)S(6)} %select_n.3), kind=kOutput, calls=%fused_computation.23 | convolution fusion | flops 201785344 | bytes 1703944 | tf_op jit(solution)/shard_map/kdr,krq->kdq/dot_general | solution.py:112
  120.7 9.2 %psum.28 = f32[]{:T(128)} all-reduce(f32[]{:T(128)} %get-tuple-element.15), channel_id=1, replica_groups=mesh['fs_0'=4,'fs_1'=4,'tp_0'=4,'tp_1'=2] {'fs_0'}, use_global_device_ids=true, to_apply=%region_5.0 | all-reduce | flops 1 | bytes 8 | tf_op jit(solution)/shard_map/psum | solution.py:50
  129.8 9.2 %psum.29 = f32[]{:T(128)} all-reduce(f32[]{:T(128)} %psum.28), channel_id=1, replica_groups=mesh['fs_0'=4,'fs_1'=4,'tp_0'=4,'tp_1'=2] {'fs_1'}, use_global_device_ids=true, to_apply=%region_6.0 | all-reduce | flops 1 | bytes 8 | tf_op jit(solution)/shard_map/psum | solution.py:50
  139.1 9.5 %psum.30 = f32[]{:T(128)} all-reduce(f32[]{:T(128)} %psum.29), channel_id=1, replica_groups=mesh['fs_0'=4,'fs_1'=4,'tp_0'=4,'tp_1'=2] {'tp_0'}, use_global_device_ids=true, to_apply=%region_7.0 | all-reduce | flops 1 | bytes 8 | tf_op jit(solution)/shard_map/psum | solution.py:50
  148.6 3.1 %psum.31 = f32[]{:T(128)} all-reduce(f32[]{:T(128)} %psum.30), channel_id=1, replica_groups=mesh['fs_0'=4,'fs_1'=4,'tp_0'=4,'tp_1'=2] {'tp_1'}, use_global_device_ids=true, to_apply=%region_8.0 | all-reduce | flops 1 | bytes 8 | tf_op jit(solution)/shard_map/psum | solution.py:50
  152.3 0.8 fusion.14
  153.2 0.2 broadcast_in_dim.12
  153.4 31.6 %all_to_all.21 = bf16[16,2,128,256]{3,2,1,0:T(8,128)(2,1)S(1)} all-to-all(bf16[16,2,128,256]{3,2,1,0:T(8,128)(2,1)S(1)} %broadcast_in_dim.12), channel_id=1, replica_groups=mesh['fs_0'=4,'fs_1'=4,'tp_0'=4,'tp_1'=2] {'fs_0','fs_1'}, dimensions={0} | all-to-all | bytes 4194304 | tf_op jit(solution)/shard_map/all_to_all | solution.py:30
  185.1 1.5 copy.20
  (21 shorter events, 0.1 us)
Async XLA Ops:
  0.6 6.1 %copy-start = (bf16[2560,256]{1,0:T(8,128)(2,1)S(1)}, bf16[2560,256]{1,0:T(8,128)(2,1)}, u32[]{:S(2)}) copy-start(bf16[2560,256]{1,0:T(8,128)(2,1)} %param.10) | copy-start | bytes 3932164
  0.6 7.7 %copy-start.5 = (bf16[2560,2048]{1,0:T(8,128)(2,1)S(1)}, bf16[2560,2048]{1,0:T(8,128)(2,1)}, u32[]{:S(2)}) copy-start(bf16[2560,2048]{1,0:T(8,128)(2,1)} %param.8) | copy-start | bytes 31457284
  0.7 12.3 %slice-start = ((s8[10485760]{0:T(1024)(128)(4,1)}), s8[4194304]{0:T(1024)(128)(4,1)S(1)}, s32[]{:S(2)}) async-start(s8[10485760]{0:T(1024)(128)(4,1)} %bitcast.53), calls=%async_computation.4 | async-start | bytes 8388608
  0.7 12.3 %slice-start.1 = ((s8[10485760]{0:T(1024)(128)(4,1)}), s8[4194304]{0:T(1024)(128)(4,1)S(1)}, s32[]{:S(2)}) async-start(s8[10485760]{0:T(1024)(128)(4,1)} %bitcast.53), calls=%async_computation.5 | async-start | bytes 8388608
  8.4 4.6 %slice-start.2 = ((s8[10485760]{0:T(1024)(128)(4,1)}), s8[2097152]{0:T(1024)(128)(4,1)S(1)}, s32[]{:S(2)}) async-start(s8[10485760]{0:T(1024)(128)(4,1)} %bitcast.53), calls=%async_computation.6 | async-start | bytes 4194304
  12.4 1.6 copy-start.4
  14.0 3.1 %copy-start.1 = (bf16[2560,256]{1,0:T(8,128)(2,1)S(1)}, bf16[2560,256]{1,0:T(8,128)(2,1)}, u32[]{:S(2)}) copy-start(bf16[2560,256]{1,0:T(8,128)(2,1)} %param.11) | copy-start | bytes 3932164
  89.0 14.9 %copy-start.2 = (f32[2,256,256]{2,1,0:T(8,128)S(1)}, f32[2,256,256]{2,1,0:T(8,128)}, u32[]{:S(2)}) copy-start(f32[2,256,256]{2,1,0:T(8,128)} %param.15) | copy-start | bytes 1572868
  89.9 14.0 %all-to-all-start.1 = ((f32[16,2,16,256]{3,2,1,0:T(8,128)}), f32[16,2,16,256]{3,2,1,0:T(8,128)S(1)}, u32[]{:S(2)}, u32[]{:S(2)}) async-start(f32[16,2,16,256]{3,2,1,0:T(8,128)} %broadcast_in_dim.10), calls=%async_computation.1 | async-start | bytes 1048576 | tf_op jit(solution)/shard_map/all_to_all | solution.py:30
  106.3 46.0 %copy-start.3 = (f32[2,128,256]{2,1,0:T(8,128)S(1)}, f32[2,128,256]{2,1,0:T(8,128)}, u32[]{:S(2)}) copy-start(f32[2,128,256]{2,1,0:T(8,128)} %param.12) | copy-start | bytes 786436
  107.1 9.8 %all-to-all-start.2 = ((f32[8,2,2]{2,1,0:T(2,128)}), f32[8,2,2]{2,1,0:T(2,128)S(1)}, u32[]{:S(2)}, u32[]{:S(2)}) async-start(f32[8,2,2]{2,1,0:T(2,128)} %broadcast_in_dim.11), calls=%async_computation.2 | async-start | bytes 16384 | tf_op jit(solution)/shard_map/all_to_all | solution.py:30
where the time goes:
time: 187 us
  blocking collectives  127 us (68%)
  matrix products  21.8 us (12%)
  waiting for transfers between devices  15.7 us (8%)
  starting transfers between devices  8.04 us (4%)
  other arithmetic  6.54 us (3%)
  local copies, waits for them, and re-layouts  5.82 us (3%)
    all_to_all x1, blocking collectives, summed_on_arrival(): lax.all_to_all(pieces, axis, split_axis=0, concat_axis=0, tiled=True)  64.4 us
    all_to_all x1, blocking collectives, sent_to_all(): return lax.all_to_all(copies, axis, split_axis=0, concat_axis=0, tiled=True)  31.6 us
    psum x4, blocking collectives, by_axis(): array = lax.psum(array, axis)  31 us
    all_to_all x2, waiting for transfers between devices, sent_to_all(): return lax.all_to_all(copies, axis, split_axis=0, concat_axis=0, tiled=True)  15.7 us
    dot_general x2, matrix products, per_device(): jnp.dot(lefts[index], factors[index], preferred_element_type=jnp.float32)  9.19 us
    all_to_all x2, starting transfers between devices, sent_to_all(): return lax.all_to_all(copies, axis, split_axis=0, concat_axis=0, tiled=True)  8.04 us
    dot_general x2, matrix products, block_terms(): lax.dot_general(columns, rights[index], (((0,), (0,)), ((), ())), preferr...  6.65 us
  transfers between devices with their start and end apart: 2, of which 2 were waited for; matrix products, arithmetic and copies ran while one was open for 0% of the time, Pallas kernels for 0%

commit v1 on v0

v1 whole, which is shorter than its diff:
```python
import jax
import jax.numpy as jnp
from jax import lax
from jax.experimental import pallas as pl
from jax.experimental.pallas import tpu as pltpu
from jax.sharding import Mesh
from jax.sharding import PartitionSpec as P

Z, X, Y, C = "fs_0", "fs_1", "tp_0", "tp_1"
FS, TP = (Z, X), (Y, C)
MESH = pl.DeviceIdType.MESH
F32, BF16 = jnp.float32, jnp.bfloat16
ORDER = (2, 1, 3, 0)


class Copies:
    def __init__(self, send_sems, recv_sems):
        self.send_sems, self.recv_sems, self.made = send_sems, recv_sems, []

    def send(self, src, dst, device):
        index = len(self.made)
        copy = pltpu.make_async_remote_copy(
            src_ref=src,
            dst_ref=dst,
            send_sem=self.send_sems.at[index],
            recv_sem=self.recv_sems.at[index],
            device_id=device,
            device_id_type=MESH,
        )
        copy.start()
        self.made.append(copy)
        return copy


COPIES = 160
LOADS = 24


def halves(value, terms):
    out = []
    for _ in range(terms - 1):
        part = value.astype(BF16)
        out.append(part)
        value = value - part.astype(F32)
    out.append(value.astype(BF16))
    return out


def folded(value):
    rows, cols = value.shape
    total = value[:, 0:128]
    for start in range(128, cols, 128):
        total = total + value[:, start : start + 128]
    return total.reshape(rows // 8, 8, 128).sum(axis=0)


def kernel(
    layer_inputs, output_cot, query_cot, head_outputs, weights, factors, first_moment, second_moment,
    new_weights, update, new_first, new_second, weight_copy,
    left, right, right_t, fact, grad, one_a, one_b, two_a, two_b,
    low_t, low_in1, low_in2, low_all, wts, mom1, mom2, out_w, out_u, gathered,
    own_p, own_f, tp_own, tp_in, fs_own, fs_in, tot_own, tot_in,
    load_sems, store_sems, send_sems, recv_sems,
):
    z, x, y, c = (lax.axis_index(name) for name in (Z, X, Y, C))
    lefts, rights = (layer_inputs, output_cot), (query_cot, head_outputs)
    coord = {Z: z, X: x, Y: y, C: c}
    axes = ((X, Z), (Z, X))

    def near(axis, delta):
        return {axis: lax.rem(coord[axis] + delta, 4)}

    def place(k, a, b):
        first, second = axes[k]
        at = {first: lax.rem(coord[first] + b, 4), second: lax.rem(coord[second] + a, 4)}
        return at[Z] * 4 + at[X]

    loads = []

    def load(pairs, whole):
        sem = load_sems.at[len(loads)]
        for src, dst in pairs:
            pltpu.make_async_copy(src, dst, sem).start()
        loads.append(pltpu.make_async_copy(whole, whole, sem))
        return loads[-1]

    def load_left(k, a):
        pairs = []
        for b in range(4):
            cols = pl.ds(pl.multiple_of(place(k, a, b) * 128, 128), 128)
            pairs.append((lefts[k].at[:, cols], left.at[k, a, :, pl.ds(128 * b, 128)]))
        return load(pairs, left.at[k, a])

    def load_factors(k):
        pairs = []
        for a in range(4):
            for b in range(4):
                rows = pl.ds(pl.multiple_of(place(k, a, b) * 128, 128), 128)
                pairs.append((factors.at[k, rows, :], fact.at[k, a, pl.ds(128 * b, 128), :]))
        return load(pairs, fact.at[k])

    right_in, left_in, fact_in = [None] * 2, {}, [None] * 2
    for k in range(2):
        right_in[k] = load([(rights[k], right.at[k])], right.at[k])
        left_in[k, ORDER[0]] = load_left(k, ORDER[0])
    for k in range(2):
        left_in[k, ORDER[1]] = load_left(k, ORDER[1])
    for k in range(2):
        fact_in[k] = load_factors(k)
    for a in ORDER[2:]:
        for k in range(2):
            left_in[k, a] = load_left(k, a)
    mom1_in = load([(first_moment, mom1)], mom1)
    mom2_in = load([(second_moment, mom2)], mom2)
    wts_in = load([(weights, wts)], wts)

    barrier = pltpu.get_barrier_semaphore()
    fs_peers = [
        {Z: lax.rem(z + dz, 4), X: lax.rem(x + dx, 4)} for dz in range(4) for dx in range(4) if dz or dx
    ]
    tp_peers = [
        {Y: lax.rem(y + dy, 4), C: lax.rem(c + dc, 2)} for dy in range(4) for dc in range(2) if dy or dc
    ]
    for peer in fs_peers + tp_peers:
        pl.semaphore_signal(barrier, inc=1, device_id=peer, device_id_type=MESH)

    copies = Copies(send_sems, recv_sems)
    top, bottom = pl.ds(0, 128), pl.ds(128, 128)

    def transpose_right(k):
        right_in[k].wait()
        for start in range(0, 2560, 256):
            right_t[k, :, start : start + 256] = right[k, start : start + 256, :].T

    def local_grad(k, a):
        left_in[k, a].wait()
        value = jnp.dot(right_t[k], left[k, a], preferred_element_type=F32)
        for b in range(4):
            grad[k, a, b] = value[:, 128 * b : 128 * b + 128]

    def local_low(k, a):
        total = None
        for b in range(4):
            block = grad[k, a, b]
            rows = fact[k, a, 128 * b : 128 * b + 128, :]
            for part in halves(block, 2):
                term = jnp.dot(part, rows, preferred_element_type=F32)
                total = term if total is None else total + term
        if a == ORDER[0]:
            low_t[k] = total
        else:
            low_t[k] = low_t[k] + total

    pending = {}

    def one_start(k, a):
        axis = axes[k][0]
        got = {}
        got["a0"] = copies.send(grad.at[k, a, 2, top], one_a.at[k, a, 0], near(axis, 1))
        got["a1"] = copies.send(grad.at[k, a, 2, bottom], one_a.at[k, a, 1], near(axis, 3))
        got["b01"] = copies.send(grad.at[k, a, 1, bottom], one_b.at[k, a, 0, 1], near(axis, 1))
        got["b10"] = copies.send(grad.at[k, a, 3, top], one_b.at[k, a, 1, 0], near(axis, 3))
        pending["one", k, a] = got

    def one_forward(k, a):
        axis = axes[k][0]
        got = pending["one", k, a]
        got["a0"].wait_recv()
        grad[k, a, 1, 0:128] = grad[k, a, 1, 0:128] + one_a[k, a, 0]
        got["b00"] = copies.send(grad.at[k, a, 1, top], one_b.at[k, a, 0, 0], near(axis, 1))
        got["a1"].wait_recv()
        grad[k, a, 3, 128:256] = grad[k, a, 3, 128:256] + one_a[k, a, 1]
        got["b11"] = copies.send(grad.at[k, a, 3, bottom], one_b.at[k, a, 1, 1], near(axis, 3))

    def one_finish(k, a):
        got = pending["one", k, a]
        got["b01"].wait_recv()
        got["b10"].wait_recv()
        got["b00"].wait_recv()
        grad[k, a, 0, 0:128] = grad[k, a, 0, 0:128] + (one_b[k, a, 0, 0] + one_b[k, a, 1, 0])
        got["b11"].wait_recv()
        grad[k, a, 0, 128:256] = grad[k, a, 0, 128:256] + (one_b[k, a, 0, 1] + one_b[k, a, 1, 1])

    def two_start(k):
        axis = axes[k][1]
        got = pending["two", k] = {}
        got["a0"] = copies.send(grad.at[k, 2, 0, top], two_a.at[k, 0], near(axis, 1))
        got["a1"] = copies.send(grad.at[k, 2, 0, bottom], two_a.at[k, 1], near(axis, 3))

    def two_plus(k):
        axis = axes[k][1]
        got = pending["two", k]
        got["b01"] = copies.send(grad.at[k, 1, 0, bottom], two_b.at[k, 0, 1], near(axis, 1))
        got["a0"].wait_recv()
        grad[k, 1, 0, 0:128] = grad[k, 1, 0, 0:128] + two_a[k, 0]
        got["b00"] = copies.send(grad.at[k, 1, 0, top], two_b.at[k, 0, 0], near(axis, 1))

    def two_minus(k):
        axis = axes[k][1]
        got = pending["two", k]
        got["b10"] = copies.send(grad.at[k, 3, 0, top], two_b.at[k, 1, 0], near(axis, 3))
        got["a1"].wait_recv()
        grad[k, 3, 0, 128:256] = grad[k, 3, 0, 128:256] + two_a[k, 1]
        got["b11"] = copies.send(grad.at[k, 3, 0, bottom], two_b.at[k, 1, 1], near(axis, 3))

    def two_finish(k):
        got = pending["two", k]
        for name in ("b01", "b10", "b00", "b11"):
            got[name].wait_recv()
        top_sum = grad[k, 0, 0, 0:128] + (two_b[k, 0, 0] + two_b[k, 1, 0])
        bottom_sum = grad[k, 0, 0, 128:256] + (two_b[k, 0, 1] + two_b[k, 1, 1])
        return jnp.concatenate([top_sum, bottom_sum], axis=0)

    def low_rows(k, b, a=None):
        first, second = axes[k]
        start = lax.rem(coord[first] + b, 4) * 64
        if a is None:
            return pl.ds(pl.multiple_of(start, 64), 64)
        return pl.ds(pl.multiple_of(start + lax.rem(coord[second] + a, 4) * 16, 16), 16)

    def low_one(k):
        pending["l1", k] = [
            copies.send(low_t.at[k, low_rows(k, b)], low_in1.at[k, 3 - b], near(axes[k][0], b)) for b in (2, 1, 3)
        ]

    def low_two(k):
        for copy in pending["l1", k]:
            copy.wait_recv()
        rows = low_rows(k, 0)
        low_t[k, rows] = low_t[k, rows] + low_in1[k, 0] + low_in1[k, 1] + low_in1[k, 2]
        pending["l2", k] = [
            copies.send(low_t.at[k, low_rows(k, 0, a)], low_in2.at[k, 3 - a], near(axes[k][1], a)) for a in (2, 1, 3)
        ]

    def low_three(k):
        for copy in pending["l2", k]:
            copy.wait_recv()
        rows = low_rows(k, 0, 0)
        low_all[k, rows] = low_t[k, rows] + low_in2[k, 0] + low_in2[k, 1] + low_in2[k, 2]
        pending["l3", k] = [
            copies.send(low_all.at[k, rows], low_all.at[k, rows], near(axes[k][1], a)) for a in (2, 1, 3)
        ]

    def low_four(k):
        for copy in pending["l3", k]:
            copy.wait_recv()
        rows = low_rows(k, 0)
        pending["l4", k] = [
            copies.send(low_all.at[k, rows], low_all.at[k, rows], near(axes[k][0], b)) for b in (2, 1, 3)
        ]

    stores = []

    def store(src, dst):
        copy = pltpu.make_async_copy(src, dst, store_sems.at[len(stores)])
        copy.start()
        stores.append(copy)

    def moments(k):
        for copy in pending["l4", k]:
            copy.wait_recv()
        low = low_all[k].T
        first = 0.9 * mom1[k] + 0.1 * low
        second = 0.95 * mom2[k] + 0.05 * low * low
        mom1[k] = first
        mom2[k] = second
        normed = first / (jnp.sqrt(second) + 1e-06)
        tp_own[k] = folded(normed * normed)
        tp_own[2 + k] = folded(low * low)
        mine = fact[k, 0, 0:128, :]
        own_p[k] = sum(jnp.dot(mine, part, preferred_element_type=F32) for part in halves(normed, 3))
        own_f[k] = sum(jnp.dot(mine, part, preferred_element_type=F32) for part in halves(low, 3))

    last = None
    for step, a in enumerate(ORDER):
        for k in range(2):
            if step == 0:
                transpose_right(k)
            local_grad(k, a)
            if step == 0 and k == 0:
                pl.semaphore_wait(barrier, len(fs_peers) + len(tp_peers))
            if step < 2:
                one_start(k, a)
            if step == 1:
                one_forward(k, ORDER[0])
        for k in range(2):
            if step == 0:
                fact_in[k].wait()
            local_low(k, a)
    for k in range(2):
        low_one(k)
    for k in range(2):
        one_forward(k, ORDER[1])
        one_start(k, ORDER[2])
        one_finish(k, ORDER[0])
        two_start(k)
    for k in range(2):
        low_two(k)
    for k in range(2):
        one_forward(k, ORDER[2])
        one_start(k, ORDER[3])
        one_finish(k, ORDER[1])
        two_plus(k)
    for k in range(2):
        low_three(k)
    for k in range(2):
        one_forward(k, ORDER[3])
        one_finish(k, ORDER[2])
        two_minus(k)
    for k in range(2):
        low_four(k)
    mom1_in.wait()
    mom2_in.wait()
    for k in range(2):
        moments(k)
    store(mom1, new_first)
    store(mom2, new_second)
    tp_copies = [copies.send(tp_own, tp_in.at[i], peer) for i, peer in enumerate(tp_peers)]
    for k in range(2):
        one_finish(k, ORDER[3])
    for copy in tp_copies:
        copy.wait_recv()
    sums = tp_own[...]
    for i in range(len(tp_peers)):
        sums = sums + tp_in[i]
    wts_in.wait()

    square = None
    for k in range(2):
        normed_sum = jnp.sum(sums[k], keepdims=True)
        low_sum = jnp.sum(sums[2 + k], keepdims=True)
        ratio = jnp.sqrt(normed_sum) / jnp.sqrt(low_sum + 1e-06)
        own = two_finish(k).T
        step = own_p[k] + ratio * (own - own_f[k])
        out_u[k] = step
        term = folded(step * step)
        square = term if square is None else square + term
    tot_own[...] = square
    tot_copies = [copies.send(tot_own, tot_in.at[i], peer) for i, peer in enumerate(tp_peers)]
    for copy in tot_copies:
        copy.wait_recv()
    for i in range(len(tp_peers)):
        square = square + tot_in[i]
    fs_own[...] = square
    fs_copies = [copies.send(fs_own, fs_in.at[i], peer) for i, peer in enumerate(fs_peers)]
    for copy in fs_copies:
        copy.wait_recv()
    for i in range(len(fs_peers)):
        square = square + fs_in[i]
    total = jnp.sum(square, keepdims=True)
    scale = lax.rsqrt(total / (2.0 * 2048 * 2048) + 1e-06)

    for k in range(2):
        value = out_u[k] * scale
        out_u[k] = value
        value = wts[k] - 0.02 * value
        out_w[k] = value
        gathered[k, 0, 0] = value.astype(BF16)
    store(out_u, update)
    store(out_w, new_weights)

    def put(k, a, b):
        rows = pl.ds(pl.multiple_of(place(k, a, b) * 128, 128), 128)
        store(gathered.at[k, a, b], weight_copy.at[k, rows, :])

    upper, lower = pl.ds(0, 64), pl.ds(64, 64)

    def spread(k, b):
        block = gathered.at[k, 0, b]
        got = pending["w", k, b] = {}
        got["plus"] = copies.send(block, gathered.at[k, 3, b], near(axes[k][1], 1))
        got["minus"] = copies.send(block, gathered.at[k, 1, b], near(axes[k][1], 3))
        put(k, 0, b)

    def relay(k, b):
        got = pending["w", k, b]
        got["plus"].wait_recv()
        got["far0"] = copies.send(gathered.at[k, 3, b, upper], gathered.at[k, 2, b, upper], near(axes[k][1], 1))
        put(k, 3, b)
        got["minus"].wait_recv()
        got["far1"] = copies.send(gathered.at[k, 1, b, lower], gathered.at[k, 2, b, lower], near(axes[k][1], 3))
        put(k, 1, b)

    def land(k, b):
        got = pending["w", k, b]
        got["far0"].wait_recv()
        got["far1"].wait_recv()
        put(k, 2, b)

    for k in range(2):
        axis = axes[k][0]
        got = pending["v", k] = {}
        got["plus"] = copies.send(gathered.at[k, 0, 0], gathered.at[k, 0, 3], near(axis, 1))
        got["minus"] = copies.send(gathered.at[k, 0, 0], gathered.at[k, 0, 1], near(axis, 3))
    for k in range(2):
        spread(k, 0)
    for k in range(2):
        axis = axes[k][0]
        got = pending["v", k]
        got["plus"].wait_recv()
        got["far0"] = copies.send(gathered.at[k, 0, 3, upper], gathered.at[k, 0, 2, upper], near(axis, 1))
        got["minus"].wait_recv()
        got["far1"] = copies.send(gathered.at[k, 0, 1, lower], gathered.at[k, 0, 2, lower], near(axis, 3))
        spread(k, 3)
        spread(k, 1)
    for k in range(2):
        relay(k, 0)
    for k in range(2):
        got = pending["v", k]
        got["far0"].wait_recv()
        got["far1"].wait_recv()
        spread(k, 2)
    for b in (3, 1, 2):
        for k in range(2):
            relay(k, b)
    for b in (0, 3, 1, 2):
        for k in range(2):
            land(k, b)
    for copy in copies.made:
        copy.wait_send()
    for copy in stores:
        copy.wait()


def per_device(*args):
    any_space = pl.BlockSpec(memory_space=pl.ANY)
    shapes = (
        ((2, 128, 256), F32),
        ((2, 128, 256), F32),
        ((2, 256, 256), F32),
        ((2, 256, 256), F32),
        ((2, 2048, 256), BF16),
    )
    dma = pltpu.SemaphoreType.DMA
    return pl.pallas_call(
        kernel,
        name="step",
        out_shape=[jax.ShapeDtypeStruct(*shape) for shape in shapes],
        in_specs=[any_space] * 8,
        out_specs=[any_space] * 5,
        scratch_shapes=[
            pltpu.VMEM((2, 4, 2560, 512), BF16),
            pltpu.VMEM((2, 2560, 256), BF16),
            pltpu.VMEM((2, 256, 2560), BF16),
            pltpu.VMEM((2, 4, 512, 256), BF16),
            pltpu.VMEM((2, 4, 4, 256, 128), F32),
            pltpu.VMEM((2, 4, 2, 128, 128), F32),
            pltpu.VMEM((2, 4, 2, 2, 128, 128), F32),
            pltpu.VMEM((2, 2, 128, 128), F32),
            pltpu.VMEM((2, 2, 2, 128, 128), F32),
            pltpu.VMEM((2, 256, 256), F32),
            pltpu.VMEM((2, 3, 64, 256), F32),
            pltpu.VMEM((2, 3, 16, 256), F32),
            pltpu.VMEM((2, 256, 256), F32),
            pltpu.VMEM((2, 128, 256), F32),
            pltpu.VMEM((2, 256, 256), F32),
            pltpu.VMEM((2, 256, 256), F32),
            pltpu.VMEM((2, 128, 256), F32),
            pltpu.VMEM((2, 128, 256), F32),
            pltpu.VMEM((2, 4, 4, 128, 256), BF16),
            pltpu.VMEM((2, 128, 256), F32),
            pltpu.VMEM((2, 128, 256), F32),
            pltpu.VMEM((4, 8, 128), F32),
            pltpu.VMEM((7, 4, 8, 128), F32),
            pltpu.VMEM((8, 128), F32),
            pltpu.VMEM((15, 8, 128), F32),
            pltpu.VMEM((8, 128), F32),
            pltpu.VMEM((7, 8, 128), F32),
            dma((LOADS,)),
            dma((40,)),
            dma((COPIES,)),
            dma((COPIES,)),
        ],
        compiler_params=pltpu.CompilerParams(
            collective_id=0, has_side_effects=True, vmem_limit_bytes=60 * 1024 * 1024
        ),
    )(*args)


def solution(mesh):
    finer = Mesh(mesh.devices.reshape(4, 4, 4, 2), (Z, X, Y, C))
    in_specs = (
        P(FS, None),
        P(FS, None),
        P(FS, TP),
        P(FS, TP),
        P(None, FS, TP),
        P(),
        P(None, None, TP),
        P(None, None, TP),
    )
    out_specs = (
        P(None, FS, TP),
        P(None, FS, TP),
        P(None, None, TP),
        P(None, None, TP),
        P(None, None, TP),
    )
    return jax.shard_map(per_device, mesh=finer, in_specs=in_specs, out_specs=out_specs, check_vma=False)
```

time: 187 us -> 85.8 us (0.46)
  blocking collectives: 127 us -> 0 us
  Pallas kernels: 0 us -> 76.1 us
  matrix products: 21.8 us -> 0 us
  waiting for transfers between devices: 15.7 us -> 0 us
  starting transfers between devices: 8.04 us -> 0 us
  other arithmetic: 6.54 us -> 0 us
  local copies, waits for them, and re-layouts: 5.82 us -> 8.55 us
    all_to_all x2 -> x0, blocking collectives: 96 us -> none  [the longest x1 64.4 us: summed_on_arrival(): lax.all_to_all(pieces, axis, split_axis=0, concat_axis=0, tiled=True)]
    pallas_call x0 -> x1, Pallas kernels: none -> 76.1 us  [per_device(): pl.pallas_call(kernel, name='step', out_shape=[jax.ShapeDtypeStruct(*shap...]
    psum x4 -> x0, blocking collectives: 31 us -> none  [by_axis(): array = lax.psum(array, axis)]
    dot_general x10 -> x0, matrix products: 21.8 us -> none  [the longest x2 9.19 us: per_device(): jnp.dot(lefts[index], factors[index], preferred_element_type=jnp.float32)]
    all_to_all x2 -> x0, waiting for transfers between devices: 15.7 us -> none  [sent_to_all(): return lax.all_to_all(copies, axis, split_axis=0, concat_axis=0, tiled=True)]
    all_to_all x2 -> x0, starting transfers between devices: 8.04 us -> none  [sent_to_all(): return lax.all_to_all(copies, axis, split_axis=0, concat_axis=0, tiled=True)]
    unnamed x18 -> x7, local copies, waits for them, and re-layouts: 2.65 us -> 8.55 us
    reduce_sum x4 -> x0, other arithmetic: 5.22 us -> none  [the longest x1 2.66 us: summed_on_arrival(): return arrived.sum(axis=0)]
  transfers between devices with their start and end apart: 2 -> 0, of which waited for: 2 -> 0; matrix products, arithmetic and copies ran while one was open for 0% -> 0% of each run, Pallas kernels for 0% -> 0%
where the time goes in v1:
time: 85.8 us; the launch traced here: 85.3 us
  Pallas kernels  76.1 us (89%)
  local copies, waits for them, and re-layouts  8.55 us (10%)
    pallas_call x1, Pallas kernels, per_device(): pl.pallas_call(kernel, name='step', out_shape=[jax.ShapeDtypeStruct(*shap...  76.1 us
    unnamed x7, local copies, waits for them, and re-layouts  8.55 us

profile of v1, /device:TPU:0, one launch (start us, length us, event | category | flops | bytes accessed | tf_op | source)
XLA Modules:
  0.0 85.3 jit_solution(2089502337949117431)
XLA Ops:
  0.6 76.1 %step.1 = (f32[2,128,256]{2,1,0:T(8,128)}, f32[2,128,256]{2,1,0:T(8,128)}, f32[2,256,256]{2,1,0:T(8,128)}, f32[2,256,256]{2,1,0:T(8,128)}, bf16[2,2048,256]{2,1,0:T(8,128)(2,1)}) custom-call(bf16[2560,2048]{1,0:T(8,128)(2,1)} %layer_inputs.1, bf16[2560,2048]{1,0:T(8,128)(2,1)} %output_cot.1, bf16[2560,256]{1,0:T(8,128)(2,1)} %query_cot.1, ...), custom_call_target="tpu_custom_call" | custom-call | tf_op jit(solution)/shard_map/step/pallas_call | solution.py:435
  76.8 0.0 copy-start
  76.8 1.8 %copy.18 = f32[2,128,256]{2,1,0:T(8,128)} copy(f32[2,128,256]{2,1,0:T(8,128)} %get-tuple-element.10) | data formatting | bytes 524288
  78.6 1.7 %copy.19 = f32[2,128,256]{2,1,0:T(8,128)} copy(f32[2,128,256]{2,1,0:T(8,128)} %get-tuple-element.11) | data formatting | bytes 524288
  80.3 1.9 %copy.20 = f32[2,256,256]{2,1,0:T(8,128)} copy(f32[2,256,256]{2,1,0:T(8,128)} %get-tuple-element.12) | data formatting | bytes 1048576
  82.1 1.9 %copy.21 = f32[2,256,256]{2,1,0:T(8,128)} copy(f32[2,256,256]{2,1,0:T(8,128)} %get-tuple-element.13) | data formatting | bytes 1048576
  84.0 0.0 copy-done
  84.0 1.3 %copy.22 = bf16[2,2048,256]{2,1,0:T(8,128)(2,1)} copy(bf16[2,2048,256]{2,1,0:T(8,128)(2,1)S(1)} %copy-done) | data formatting | bytes 4194304
Async XLA Ops:
  76.8 7.2 %copy-start = (bf16[2,2048,256]{2,1,0:T(8,128)(2,1)S(1)}, bf16[2,2048,256]{2,1,0:T(8,128)(2,1)}, u32[]{:S(2)}) copy-start(bf16[2,2048,256]{2,1,0:T(8,128)(2,1)} %get-tuple-element.14) | copy-start | bytes 6291460

commit v2 on v1

--- a/solution.py
+++ b/solution.py
@@ -32,7 +32,7 @@
         return copy
 
 
-COPIES = 160
+COPIES = 192
 LOADS = 24
 
 
@@ -56,11 +56,11 @@
 
 def kernel(
     layer_inputs, output_cot, query_cot, head_outputs, weights, factors, first_moment, second_moment,
-    new_weights, update, new_first, new_second, weight_copy,
+    out_w, out_u, out_1, out_2, gathered,
     left, right, right_t, fact, grad, one_a, one_b, two_a, two_b,
-    low_t, low_in1, low_in2, low_all, wts, mom1, mom2, out_w, out_u, gathered,
-    own_p, own_f, tp_own, tp_in, fs_own, fs_in, tot_own, tot_in,
-    load_sems, store_sems, send_sems, recv_sems,
+    low_t, low_a, low_b, low_in, low_all, wts, mom1, mom2,
+    own_p, own_f, tp_own, tp_in, tot_own, tot_in, last_own, last_in,
+    load_sems, send_sems, recv_sems,
 ):
     z, x, y, c = (lax.axis_index(name) for name in (Z, X, Y, C))
     lefts, rights = (layer_inputs, output_cot), (query_cot, head_outputs)
@@ -211,59 +211,83 @@
         bottom_sum = grad[k, 0, 0, 128:256] + (two_b[k, 0, 1] + two_b[k, 1, 1])
         return jnp.concatenate([top_sum, bottom_sum], axis=0)
 
-    def low_rows(k, b, a=None):
+    def low_rows(k, b, half=None):
+        start = lax.rem(coord[axes[k][0]] + b, 4) * 64
+        if half is None:
+            return pl.ds(pl.multiple_of(start, 64), 64)
+        return pl.ds(pl.multiple_of(start + 32 * half, 32), 32)
+
+    def low_piece(k, a):
         first, second = axes[k]
-        start = lax.rem(coord[first] + b, 4) * 64
-        if a is None:
-            return pl.ds(pl.multiple_of(start, 64), 64)
-        return pl.ds(pl.multiple_of(start + lax.rem(coord[second] + a, 4) * 16, 16), 16)
-
-    def low_one(k):
-        pending["l1", k] = [
-            copies.send(low_t.at[k, low_rows(k, b)], low_in1.at[k, 3 - b], near(axes[k][0], b)) for b in (2, 1, 3)
+        return pl.ds(pl.multiple_of(coord[first] * 64 + lax.rem(coord[second] + a, 4) * 16, 16), 16)
+
+    def low_start(k):
+        axis = axes[k][0]
+        got = pending["low", k] = {}
+        got["a0"] = copies.send(low_t.at[k, low_rows(k, 2, 0)], low_a.at[k, 0], near(axis, 1))
+        got["a1"] = copies.send(low_t.at[k, low_rows(k, 2, 1)], low_a.at[k, 1], near(axis, 3))
+        got["b01"] = copies.send(low_t.at[k, low_rows(k, 1, 1)], low_b.at[k, 0, 1], near(axis, 1))
+        got["b10"] = copies.send(low_t.at[k, low_rows(k, 3, 0)], low_b.at[k, 1, 0], near(axis, 3))
+
+    def low_forward(k):
+        axis = axes[k][0]
+        got = pending["low", k]
+        got["a0"].wait_recv()
+        rows = low_rows(k, 1, 0)
+        low_t[k, rows] = low_t[k, rows] + low_a[k, 0]
+        got["b00"] = copies.send(low_t.at[k, rows], low_b.at[k, 0, 0], near(axis, 1))
+        got["a1"].wait_recv()
+        rows = low_rows(k, 3, 1)
+        low_t[k, rows] = low_t[k, rows] + low_a[k, 1]
+        got["b11"] = copies.send(low_t.at[k, rows], low_b.at[k, 1, 1], near(axis, 3))
+
+    def low_second(k):
+        got = pending["low", k]
+        for name in ("b01", "b10", "b00", "b11"):
+            got[name].wait_recv()
+        for half in range(2):
+            rows = low_rows(k, 0, half)
+            low_t[k, rows] = low_t[k, rows] + (low_b[k, 0, half] + low_b[k, 1, half])
+        pending["low2", k] = [
+            copies.send(low_t.at[k, low_piece(k, a)], low_in.at[k, 3 - a], near(axes[k][1], a)) for a in (2, 1, 3)
         ]
 
-    def low_two(k):
-        for copy in pending["l1", k]:
+    def low_third(k):
+        for copy in pending["low2", k]:
             copy.wait_recv()
-        rows = low_rows(k, 0)
-        low_t[k, rows] = low_t[k, rows] + low_in1[k, 0] + low_in1[k, 1] + low_in1[k, 2]
-        pending["l2", k] = [
-            copies.send(low_t.at[k, low_rows(k, 0, a)], low_in2.at[k, 3 - a], near(axes[k][1], a)) for a in (2, 1, 3)
-        ]
-
-    def low_three(k):
-        for copy in pending["l2", k]:
-            copy.wait_recv()
-        rows = low_rows(k, 0, 0)
-        low_all[k, rows] = low_t[k, rows] + low_in2[k, 0] + low_in2[k, 1] + low_in2[k, 2]
-        pending["l3", k] = [
+        rows = low_piece(k, 0)
+        low_all[k, rows] = low_t[k, rows] + low_in[k, 0] + low_in[k, 1] + low_in[k, 2]
+        pending["low3", k] = [
             copies.send(low_all.at[k, rows], low_all.at[k, rows], near(axes[k][1], a)) for a in (2, 1, 3)
         ]
 
-    def low_four(k):
-        for copy in pending["l3", k]:
+    def low_fourth(k):
+        for copy in pending["low3", k]:
             copy.wait_recv()
+        axis = axes[k][0]
         rows = low_rows(k, 0)
-        pending["l4", k] = [
-            copies.send(low_all.at[k, rows], low_all.at[k, rows], near(axes[k][0], b)) for b in (2, 1, 3)
-        ]
-
-    stores = []
-
-    def store(src, dst):
-        copy = pltpu.make_async_copy(src, dst, store_sems.at[len(stores)])
-        copy.start()
-        stores.append(copy)
+        got = pending["low4", k] = {}
+        got["plus"] = copies.send(low_all.at[k, rows], low_all.at[k, rows], near(axis, 1))
+        got["minus"] = copies.send(low_all.at[k, rows], low_all.at[k, rows], near(axis, 3))
+
+    def low_fifth(k):
+        axis = axes[k][0]
+        got = pending["low4", k]
+        got["plus"].wait_recv()
+        rows = low_rows(k, 3, 0)
+        got["far0"] = copies.send(low_all.at[k, rows], low_all.at[k, rows], near(axis, 1))
+        got["minus"].wait_recv()
+        rows = low_rows(k, 1, 1)
+        got["far1"] = copies.send(low_all.at[k, rows], low_all.at[k, rows], near(axis, 3))
 
     def moments(k):
-        for copy in pending["l4", k]:
-            copy.wait_recv()
+        pending["low4", k]["far0"].wait_recv()
+        pending["low4", k]["far1"].wait_recv()
         low = low_all[k].T
         first = 0.9 * mom1[k] + 0.1 * low
         second = 0.95 * mom2[k] + 0.05 * low * low
-        mom1[k] = first
-        mom2[k] = second
+        out_1[k] = first
+        out_2[k] = second
         normed = first / (jnp.sqrt(second) + 1e-06)
         tp_own[k] = folded(normed * normed)
         tp_own[2 + k] = folded(low * low)
@@ -271,84 +295,100 @@
         own_p[k] = sum(jnp.dot(mine, part, preferred_element_type=F32) for part in halves(normed, 3))
         own_f[k] = sum(jnp.dot(mine, part, preferred_element_type=F32) for part in halves(low, 3))
 
-    last = None
-    for step, a in enumerate(ORDER):
-        for k in range(2):
-            if step == 0:
-                transpose_right(k)
-            local_grad(k, a)
-            if step == 0 and k == 0:
-                pl.semaphore_wait(barrier, len(fs_peers) + len(tp_peers))
-            if step < 2:
-                one_start(k, a)
-            if step == 1:
-                one_forward(k, ORDER[0])
-        for k in range(2):
-            if step == 0:
-                fact_in[k].wait()
-            local_low(k, a)
-    for k in range(2):
-        low_one(k)
-    for k in range(2):
-        one_forward(k, ORDER[1])
-        one_start(k, ORDER[2])
-        one_finish(k, ORDER[0])
+    both = range(2)
+    c0, c1, c2, c3 = ORDER
+    for k in both:
+        transpose_right(k)
+        local_grad(k, c0)
+        if k == 0:
+            pl.semaphore_wait(barrier, len(fs_peers) + len(tp_peers))
+        one_start(k, c0)
+    for k in both:
+        fact_in[k].wait()
+        local_low(k, c0)
+    for k in both:
+        local_grad(k, c1)
+        one_forward(k, c0)
+        one_start(k, c1)
+    for k in both:
+        local_low(k, c1)
+        local_grad(k, c2)
+    for k in both:
+        local_low(k, c2)
+        local_grad(k, c3)
+        one_forward(k, c1)
+        one_start(k, c2)
+    for k in both:
+        local_low(k, c3)
+        low_start(k)
+    for k in both:
+        one_finish(k, c0)
         two_start(k)
-    for k in range(2):
-        low_two(k)
-    for k in range(2):
-        one_forward(k, ORDER[2])
-        one_start(k, ORDER[3])
-        one_finish(k, ORDER[1])
+    for k in both:
+        one_forward(k, c2)
+    for k in both:
+        low_forward(k)
+        one_start(k, c3)
+    for k in both:
+        one_finish(k, c1)
         two_plus(k)
-    for k in range(2):
-        low_three(k)
-    for k in range(2):
-        one_forward(k, ORDER[3])
-        one_finish(k, ORDER[2])
+    for k in both:
+        low_second(k)
+    for k in both:
+        one_forward(k, c3)
+    for k in both:
+        low_third(k)
+    for k in both:
+        one_finish(k, c2)
         two_minus(k)
-    for k in range(2):
-        low_four(k)
+    for k in both:
+        low_fourth(k)
+    for k in both:
+        one_finish(k, c3)
+    for k in both:
+        low_fifth(k)
     mom1_in.wait()
     mom2_in.wait()
-    for k in range(2):
+    wts_in.wait()
+    for k in both:
         moments(k)
-    store(mom1, new_first)
-    store(mom2, new_second)
     tp_copies = [copies.send(tp_own, tp_in.at[i], peer) for i, peer in enumerate(tp_peers)]
-    for k in range(2):
-        one_finish(k, ORDER[3])
+    tot_own[6:8, :] = jnp.zeros((2, 128), F32)
+    for k in both:
+        resid = two_finish(k).T - own_f[k]
+        own_f[k] = resid
+        parts = (own_p[k] * own_p[k], own_p[k] * resid, resid * resid)
+        for i, part in enumerate(parts):
+            tot_own[3 * k + i : 3 * k + i + 1, :] = folded(part).sum(axis=0, keepdims=True)
+    tot_copies = [copies.send(tot_own, tot_in.at[i], peer) for i, peer in enumerate(fs_peers)]
     for copy in tp_copies:
         copy.wait_recv()
     sums = tp_own[...]
     for i in range(len(tp_peers)):
         sums = sums + tp_in[i]
-    wts_in.wait()
-
-    square = None
-    for k in range(2):
-        normed_sum = jnp.sum(sums[k], keepdims=True)
-        low_sum = jnp.sum(sums[2 + k], keepdims=True)
-        ratio = jnp.sqrt(normed_sum) / jnp.sqrt(low_sum + 1e-06)
-        own = two_finish(k).T
-        step = own_p[k] + ratio * (own - own_f[k])
-        out_u[k] = step
-        term = folded(step * step)
-        square = term if square is None else square + term
-    tot_own[...] = square
-    tot_copies = [copies.send(tot_own, tot_in.at[i], peer) for i, peer in enumerate(tp_peers)]
+    ratios = [
+        jnp.sqrt(jnp.sum(sums[k], keepdims=True)) / jnp.sqrt(jnp.sum(sums[2 + k], keepdims=True) + 1e-06)
+        for k in both
+    ]
+    for k in both:
+        out_u[k] = own_p[k] + ratios[k] * own_f[k]
     for copy in tot_copies:
         copy.wait_recv()
+    parts = tot_own[...]
+    for i in range(len(fs_peers)):
+        parts = parts + tot_in[i]
+    last_own[...] = parts
+    last_copies = [copies.send(last_own, last_in.at[i], peer) for i, peer in enumerate(tp_peers)]
+    for copy in last_copies:
+        copy.wait_recv()
     for i in range(len(tp_peers)):
-        square = square + tot_in[i]
-    fs_own[...] = square
-    fs_copies = [copies.send(fs_own, fs_in.at[i], peer) for i, peer in enumerate(fs_peers)]
-    for copy in fs_copies:
-        copy.wait_recv()
-    for i in range(len(fs_peers)):
-        square = square + fs_in[i]
-    total = jnp.sum(square, keepdims=True)
-    scale = lax.rsqrt(total / (2.0 * 2048 * 2048) + 1e-06)
+        parts = parts + last_in[i]
+    total = None
+    for k in both:
+        square = parts[3 * k : 3 * k + 1]
+        square = square + ratios[k] * (2.0 * parts[3 * k + 1 : 3 * k + 2] + ratios[k] * parts[3 * k + 2 : 3 * k + 3])
+        total = square if total is None else total + square
+    scale = lax.rsqrt(jnp.sum(total, keepdims=True) / (2.0 * 2048 * 2048) + 1e-06)
 
     for k in range(2):
         value = out_u[k] * scale
@@ -356,12 +396,6 @@
         value = wts[k] - 0.02 * value
         out_w[k] = value
         gathered[k, 0, 0] = value.astype(BF16)
-    store(out_u, update)
-    store(out_w, new_weights)
-
-    def put(k, a, b):
-        rows = pl.ds(pl.multiple_of(place(k, a, b) * 128, 128), 128)
-        store(gathered.at[k, a, b], weight_copy.at[k, rows, :])
 
     upper, lower = pl.ds(0, 64), pl.ds(64, 64)
 
@@ -370,22 +404,18 @@
         got = pending["w", k, b] = {}
         got["plus"] = copies.send(block, gathered.at[k, 3, b], near(axes[k][1], 1))
         got["minus"] = copies.send(block, gathered.at[k, 1, b], near(axes[k][1], 3))
-        put(k, 0, b)
 
     def relay(k, b):
         got = pending["w", k, b]
         got["plus"].wait_recv()
         got["far0"] = copies.send(gathered.at[k, 3, b, upper], gathered.at[k, 2, b, upper], near(axes[k][1], 1))
-        put(k, 3, b)
         got["minus"].wait_recv()
         got["far1"] = copies.send(gathered.at[k, 1, b, lower], gathered.at[k, 2, b, lower], near(axes[k][1], 3))
-        put(k, 1, b)
 
     def land(k, b):
         got = pending["w", k, b]
         got["far0"].wait_recv()
         got["far1"].wait_recv()
-        put(k, 2, b)
 
     for k in range(2):
         axis = axes[k][0]
@@ -418,26 +448,45 @@
             land(k, b)
     for copy in copies.made:
         copy.wait_send()
-    for copy in stores:
+
+
+def write_out(
+    out_w, out_u, out_1, out_2, gathered, new_weights, update, new_first, new_second, weight_copy, sems
+):
+    z, x = lax.axis_index(Z), lax.axis_index(X)
+    pairs = []
+    for a in range(4):
+        for b in range(4):
+            for k in range(2):
+                dz, dx = (a, b) if k == 0 else (b, a)
+                block = lax.rem(z + dz, 4) * 4 + lax.rem(x + dx, 4)
+                rows = pl.ds(pl.multiple_of(block * 128, 128), 128)
+                pairs.append((gathered.at[k, a, b], weight_copy.at[k, rows, :]))
+    pairs += [(out_1, new_first), (out_2, new_second), (out_w, new_weights), (out_u, update)]
+    copies = [pltpu.make_async_copy(*pair, sems.at[i]) for i, pair in enumerate(pairs)]
+    for copy in copies:
+        copy.start()
+    for copy in copies:
         copy.wait()
 
 
 def per_device(*args):
     any_space = pl.BlockSpec(memory_space=pl.ANY)
-    shapes = (
+    vmem_space = pl.BlockSpec(memory_space=pltpu.VMEM)
+    held = (
         ((2, 128, 256), F32),
         ((2, 128, 256), F32),
         ((2, 256, 256), F32),
         ((2, 256, 256), F32),
-        ((2, 2048, 256), BF16),
+        ((2, 4, 4, 128, 256), BF16),
     )
     dma = pltpu.SemaphoreType.DMA
-    return pl.pallas_call(
+    results = pl.pallas_call(
         kernel,
         name="step",
-        out_shape=[jax.ShapeDtypeStruct(*shape) for shape in shapes],
+        out_shape=[pltpu.VMEM(*shape) for shape in held],
         in_specs=[any_space] * 8,
-        out_specs=[any_space] * 5,
+        out_specs=[vmem_space] * 5,
         scratch_shapes=[
             pltpu.VMEM((2, 4, 2560, 512), BF16),
             pltpu.VMEM((2, 2560, 256), BF16),
@@ -449,15 +498,13 @@
             pltpu.VMEM((2, 2, 128, 128), F32),
             pltpu.VMEM((2, 2, 2, 128, 128), F32),
             pltpu.VMEM((2, 256, 256), F32),
-            pltpu.VMEM((2, 3, 64, 256), F32),
+            pltpu.VMEM((2, 2, 32, 256), F32),
+            pltpu.VMEM((2, 2, 2, 32, 256), F32),
             pltpu.VMEM((2, 3, 16, 256), F32),
             pltpu.VMEM((2, 256, 256), F32),
             pltpu.VMEM((2, 128, 256), F32),
             pltpu.VMEM((2, 256, 256), F32),
             pltpu.VMEM((2, 256, 256), F32),
-            pltpu.VMEM((2, 128, 256), F32),
-            pltpu.VMEM((2, 128, 256), F32),
-            pltpu.VMEM((2, 4, 4, 128, 256), BF16),
             pltpu.VMEM((2, 128, 256), F32),
             pltpu.VMEM((2, 128, 256), F32),
             pltpu.VMEM((4, 8, 128), F32),
@@ -467,7 +514,6 @@
             pltpu.VMEM((8, 128), F32),
             pltpu.VMEM((7, 8, 128), F32),
             dma((LOADS,)),
-            dma((40,)),
             dma((COPIES,)),
             dma((COPIES,)),
         ],
@@ -475,6 +521,16 @@
             collective_id=0, has_side_effects=True, vmem_limit_bytes=60 * 1024 * 1024
         ),
     )(*args)
+    return pl.pallas_call(
+        write_out,
+        name="write_out",
+        out_shape=[jax.ShapeDtypeStruct(shape, kind) for shape, kind in held[:4]]
+        + [jax.ShapeDtypeStruct((2, 2048, 256), BF16)],
+        in_specs=[vmem_space] * 5,
+        out_specs=[any_space] * 5,
+        scratch_shapes=[dma((36,))],
+        compiler_params=pltpu.CompilerParams(vmem_limit_bytes=1024 * 1024),
+    )(*results)
 
 
 def solution(mesh):

time: 85.8 us -> 81.3 us (0.948)
  local copies, waits for them, and re-layouts: 8.55 us -> 0 us
  Pallas kernels: 76.1 us -> 80.6 us
    unnamed x7 -> x0, local copies, waits for them, and re-layouts: 8.55 us -> none
    pallas_call x1 -> x2, Pallas kernels: 76.1 us -> 80.6 us  [the longest x1 78.4 us: per_device(): pl.pallas_call(kernel, name='step', out_shape=[pltpu.VMEM(*shape) for sha...]
where the time goes in v2:
time: 81.3 us; the launch traced here: 81.2 us
  Pallas kernels  80.6 us (99%)
    pallas_call x1, Pallas kernels, per_device(): pl.pallas_call(kernel, name='step', out_shape=[pltpu.VMEM(*shape) for sha...  78.4 us
    pallas_call x1, Pallas kernels, per_device(): pl.pallas_call(write_out, name='write_out', out_shape=[jax.ShapeDtypeStru...  2.15 us

profile of v2, /device:TPU:0, one launch (start us, length us, event | category | flops | bytes accessed | tf_op | source)
XLA Modules:
  0.0 81.2 jit_solution(14326574549772137453)
XLA Ops:
  0.6 78.4 %step.1 = (f32[2,128,256]{2,1,0:T(8,128)S(1)}, f32[2,128,256]{2,1,0:T(8,128)S(1)}, f32[2,256,256]{2,1,0:T(8,128)S(1)}, f32[2,256,256]{2,1,0:T(8,128)S(1)}, bf16[2,4,4,128,256]{4,3,2,1,0:T(8,128)(2,1)S(1)}) custom-call(bf16[2560,2048]{1,0:T(8,128)(2,1)} %layer_inputs.1, bf16[2560,2048]{1,0:T(8,128)(2,1)} %output_cot.1, bf16[2560,256]{1,0:T(8,128)(2,1)} %query_cot.1, ...), custom_call_target="tpu_custom_call" | custom-call | tf_op jit(solution)/shard_map/step/pallas_call | solution.py:484
  79.1 2.1 %write_out.1 = (f32[2,128,256]{2,1,0:T(8,128)}, f32[2,128,256]{2,1,0:T(8,128)}, f32[2,256,256]{2,1,0:T(8,128)}, f32[2,256,256]{2,1,0:T(8,128)}, bf16[2,2048,256]{2,1,0:T(8,128)(2,1)}) custom-call(f32[2,128,256]{2,1,0:T(8,128)S(1)} %get-tuple-element.10.out_w, f32[2,128,256]{2,1,0:T(8,128)S(1)} %get-tuple-element.11.out_u, ...), custom_call_target="tpu_custom_call" | custom-call | tf_op jit(solution)/shard_map/write_out/pallas_call | solution.py:524

commit v3 on v2

v3 whole, which is shorter than its diff:
```python
import math

import jax
import jax.numpy as jnp
from jax import lax
from jax.experimental import pallas as pl
from jax.experimental.pallas import tpu as pltpu
from jax.sharding import Mesh
from jax.sharding import PartitionSpec as P

Z, X, Y, C = "fs_0", "fs_1", "tp_0", "tp_1"
FS, TP = (Z, X), (Y, C)
MESH = pl.DeviceIdType.MESH
F32, BF16 = jnp.float32, jnp.bfloat16
ORDER = (2, 1, 3, 0)


class Copies:
    def __init__(self, send_sems, recv_sems, spare):
        self.send_sems, self.recv_sems, self.spare = send_sems, recv_sems, spare
        self.landings, self.sent = 0, [0]

    def landing(self):
        self.landings += 1
        return self.landings - 1

    def send(self, src, dst, device, landing):
        size = math.prod(src.shape) * src.dtype.itemsize // 1024
        if self.sent[-1] + size > self.spare.shape[0]:
            self.sent.append(0)
        self.sent[-1] += size
        pltpu.make_async_remote_copy(
            src_ref=src,
            dst_ref=dst,
            send_sem=self.send_sems.at[len(self.sent) - 1],
            recv_sem=self.recv_sems.at[landing],
            device_id=device,
            device_id_type=MESH,
        ).start()

    def wait(self, landing, place):
        pltpu.make_async_copy(place, place, self.recv_sems.at[landing]).wait()

    def wait_sent(self):
        for index, size in enumerate(self.sent):
            rows = self.spare.at[pl.ds(0, size)]
            pltpu.make_async_copy(rows, rows, self.send_sems.at[index]).wait()


SENDS, LANDINGS, LOADS = 3, 73, 15


def halves(value, terms):
    out = []
    for _ in range(terms - 1):
        part = value.astype(BF16)
        out.append(part)
        value = value - part.astype(F32)
    out.append(value.astype(BF16))
    return out


def folded(value):
    rows, cols = value.shape
    total = value[:, 0:128]
    for start in range(128, cols, 128):
        total = total + value[:, start : start + 128]
    return total.reshape(rows // 8, 8, 128).sum(axis=0)


def kernel(
    layer_inputs, output_cot, query_cot, head_outputs, weights, factors, first_moment, second_moment,
    out_w, out_u, out_1, out_2, gathered,
    left, right, right_t, fact, grad, one_a, one_b, two_a, two_b,
    low_t, low_a, low_b, low_in, low_all, wts, mom1, mom2,
    own_p, own_f, tp_own, tp_in, tot_own, tot_in, last_own, last_in,
    load_sems, send_sems, recv_sems,
):
    z, x, y, c = (lax.axis_index(name) for name in (Z, X, Y, C))
    lefts, rights = (layer_inputs, output_cot), (query_cot, head_outputs)
    coord = {Z: z, X: x, Y: y, C: c}
    axes = ((X, Z), (Z, X))

    def near(axis, delta):
        return {axis: lax.rem(coord[axis] + delta, 4)}

    def place(k, a, b):
        first, second = axes[k]
        at = {first: lax.rem(coord[first] + b, 4), second: lax.rem(coord[second] + a, 4)}
        return at[Z] * 4 + at[X]

    loads = []

    def load(pairs, whole):
        sem = load_sems.at[len(loads)]
        for src, dst in pairs:
            pltpu.make_async_copy(src, dst, sem).start()
        loads.append(pltpu.make_async_copy(whole, whole, sem))
        return loads[-1]

    def load_left(k, a):
        pairs = []
        for b in range(4):
            cols = pl.ds(pl.multiple_of(place(k, a, b) * 128, 128), 128)
            pairs.append((lefts[k].at[:, cols], left.at[k, a, :, pl.ds(128 * b, 128)]))
        return load(pairs, left.at[k, a])

    def load_factors(k):
        pairs = []
        for a in range(4):
            for b in range(4):
                rows = pl.ds(pl.multiple_of(place(k, a, b) * 128, 128), 128)
                pairs.append((factors.at[k, rows, :], fact.at[k, a, pl.ds(128 * b, 128), :]))
        return load(pairs, fact.at[k])

    right_in, left_in, fact_in = [None] * 2, {}, [None] * 2
    for k in range(2):
        right_in[k] = load([(rights[k], right.at[k])], right.at[k])
        left_in[k, ORDER[0]] = load_left(k, ORDER[0])
    for k in range(2):
        left_in[k, ORDER[1]] = load_left(k, ORDER[1])
    for k in range(2):
        fact_in[k] = load_factors(k)
    for a in ORDER[2:]:
        for k in range(2):
            left_in[k, a] = load_left(k, a)
    mom1_in = load([(first_moment, mom1)], mom1)
    mom2_in = load([(second_moment, mom2)], mom2)
    wts_in = load([(weights, wts)], wts)

    barrier = pltpu.get_barrier_semaphore()
    fs_peers = [
        {Z: lax.rem(z + dz, 4), X: lax.rem(x + dx, 4)} for dz in range(4) for dx in range(4) if dz or dx
    ]
    tp_peers = [
        {Y: lax.rem(y + dy, 4), C: lax.rem(c + dc, 2)} for dy in range(4) for dc in range(2) if dy or dc
    ]
    for peer in fs_peers + tp_peers:
        pl.semaphore_signal(barrier, inc=1, device_id=peer, device_id_type=MESH)

    copies = Copies(send_sems, recv_sems, left.at[0, 0])
    top, bottom = pl.ds(0, 128), pl.ds(128, 128)

    def transpose_right(k):
        right_in[k].wait()
        for start in range(0, 2560, 256):
            right_t[k, :, start : start + 256] = right[k, start : start + 256, :].T

    def local_grad(k, a):
        left_in[k, a].wait()
        value = jnp.dot(right_t[k], left[k, a], preferred_element_type=F32)
        for b in range(4):
            grad[k, a, b] = value[:, 128 * b : 128 * b + 128]

    def local_low(k, a):
        total = None
        value = jnp.concatenate([grad[k, a, b] for b in range(4)], axis=1)
        for part in halves(value, 2):
            term = jnp.dot(part, fact[k, a], preferred_element_type=F32)
            total = term if total is None else total + term
        if a == ORDER[0]:
            low_t[k] = total
        else:
            low_t[k] = low_t[k] + total

    pending = {}

    def opening(key, axis, far, minus, plus, into_a, into_b):
        marks = pending[key] = [copies.landing() for _ in range(3)]
        copies.send(far[0], into_a.at[0], near(axis, 1), marks[0])
        copies.send(far[1], into_a.at[1], near(axis, 3), marks[1])
        copies.send(plus[1], into_b.at[0, 1], near(axis, 1), marks[2])
        copies.send(minus[0], into_b.at[1, 0], near(axis, 3), marks[2])

    def one_start(k, a):
        far, plus, minus = ((grad.at[k, a, b, top], grad.at[k, a, b, bottom]) for b in (2, 1, 3))
        opening(("one", k, a), axes[k][0], far, minus, plus, one_a.at[k, a], one_b.at[k, a])

    def one_forward(k, a):
        axis, marks = axes[k][0], pending["one", k, a]
        copies.wait(marks[0], one_a.at[k, a, 0])
        grad[k, a, 1, 0:128] = grad[k, a, 1, 0:128] + one_a[k, a, 0]
        copies.send(grad.at[k, a, 1, top], one_b.at[k, a, 0, 0], near(axis, 1), marks[2])
        copies.wait(marks[1], one_a.at[k, a, 1])
        grad[k, a, 3, 128:256] = grad[k, a, 3, 128:256] + one_a[k, a, 1]
        copies.send(grad.at[k, a, 3, bottom], one_b.at[k, a, 1, 1], near(axis, 3), marks[2])

    def one_finish(k, a):
        copies.wait(pending["one", k, a][2], one_b.at[k, a])
        grad[k, a, 0, 0:128] = grad[k, a, 0, 0:128] + (one_b[k, a, 0, 0] + one_b[k, a, 1, 0])
        grad[k, a, 0, 128:256] = grad[k, a, 0, 128:256] + (one_b[k, a, 0, 1] + one_b[k, a, 1, 1])

    def two_start(k):
        axis = axes[k][1]
        marks = pending["two", k] = [copies.landing() for _ in range(3)]
        copies.send(grad.at[k, 2, 0, top], two_a.at[k, 0], near(axis, 1), marks[0])
        copies.send(grad.at[k, 2, 0, bottom], two_a.at[k, 1], near(axis, 3), marks[1])

    def two_plus(k):
        axis, marks = axes[k][1], pending["two", k]
        copies.send(grad.at[k, 1, 0, bottom], two_b.at[k, 0, 1], near(axis, 1), marks[2])
        copies.wait(marks[0], two_a.at[k, 0])
        grad[k, 1, 0, 0:128] = grad[k, 1, 0, 0:128] + two_a[k, 0]
        copies.send(grad.at[k, 1, 0, top], two_b.at[k, 0, 0], near(axis, 1), marks[2])

    def two_minus(k):
        axis, marks = axes[k][1], pending["two", k]
        copies.send(grad.at[k, 3, 0, top], two_b.at[k, 1, 0], near(axis, 3), marks[2])
        copies.wait(marks[1], two_a.at[k, 1])
        grad[k, 3, 0, 128:256] = grad[k, 3, 0, 128:256] + two_a[k, 1]
        copies.send(grad.at[k, 3, 0, bottom], two_b.at[k, 1, 1], near(axis, 3), marks[2])

    def two_finish(k):
        copies.wait(pending["two", k][2], two_b.at[k])
        top_sum = grad[k, 0, 0, 0:128] + (two_b[k, 0, 0] + two_b[k, 1, 0])
        bottom_sum = grad[k, 0, 0, 128:256] + (two_b[k, 0, 1] + two_b[k, 1, 1])
        return jnp.concatenate([top_sum, bottom_sum], axis=0)

    def low_rows(k, b, half=None):
        start = lax.rem(coord[axes[k][0]] + b, 4) * 64
        if half is None:
            return pl.ds(pl.multiple_of(start, 64), 64)
        return pl.ds(pl.multiple_of(start + 32 * half, 32), 32)

    def low_piece(k, a):
        first, second = axes[k]
        return pl.ds(pl.multiple_of(coord[first] * 64 + lax.rem(coord[second] + a, 4) * 16, 16), 16)

    def low_start(k):
        far, plus, minus = ([low_t.at[k, low_rows(k, b, half)] for half in range(2)] for b in (2, 1, 3))
        opening(("low", k), axes[k][0], far, minus, plus, low_a.at[k], low_b.at[k])

    def low_forward(k):
        axis, marks = axes[k][0], pending["low", k]
        copies.wait(marks[0], low_a.at[k, 0])
        rows = low_rows(k, 1, 0)
        low_t[k, rows] = low_t[k, rows] + low_a[k, 0]
        copies.send(low_t.at[k, rows], low_b.at[k, 0, 0], near(axis, 1), marks[2])
        copies.wait(marks[1], low_a.at[k, 1])
        rows = low_rows(k, 3, 1)
        low_t[k, rows] = low_t[k, rows] + low_a[k, 1]
        copies.send(low_t.at[k, rows], low_b.at[k, 1, 1], near(axis, 3), marks[2])

    def low_second(k):
        copies.wait(pending["low", k][2], low_b.at[k])
        for half in range(2):
            rows = low_rows(k, 0, half)
            low_t[k, rows] = low_t[k, rows] + (low_b[k, 0, half] + low_b[k, 1, half])
        mark = pending["low2", k] = copies.landing()
        for a in (2, 1, 3):
            copies.send(low_t.at[k, low_piece(k, a)], low_in.at[k, 3 - a], near(axes[k][1], a), mark)

    def low_third(k):
        copies.wait(pending["low2", k], low_in.at[k])
        rows = low_piece(k, 0)
        low_all[k, rows] = low_t[k, rows] + low_in[k, 0] + low_in[k, 1] + low_in[k, 2]
        mark = pending["low3", k] = copies.landing()
        for peer in fs_peers:
            copies.send(low_all.at[k, rows], low_all.at[k, rows], peer, mark)

    def moments(k):
        copies.wait(pending["low3", k], low_all.at[k, pl.ds(0, 240)])
        low = low_all[k].T
        first = 0.9 * mom1[k] + 0.1 * low
        second = 0.95 * mom2[k] + 0.05 * low * low
        out_1[k] = first
        out_2[k] = second
        normed = first / (jnp.sqrt(second) + 1e-06)
        tp_own[k] = folded(normed * normed)
        tp_own[2 + k] = folded(low * low)
        mine = fact[k, 0, 0:128, :]
        own_p[k] = sum(jnp.dot(mine, part, preferred_element_type=F32) for part in halves(normed, 3))
        own_f[k] = sum(jnp.dot(mine, part, preferred_element_type=F32) for part in halves(low, 3))

    both = range(2)
    c0, c1, c2, c3 = ORDER
    for k in both:
        transpose_right(k)
        local_grad(k, c0)
        if k == 0:
            pl.semaphore_wait(barrier, len(fs_peers) + len(tp_peers))
        one_start(k, c0)
    for k in both:
        local_grad(k, c1)
    for k in both:
        fact_in[k].wait()
        local_low(k, c0)
        one_forward(k, c0)
        one_start(k, c1)
    for k in both:
        local_low(k, c1)
    for k in both:
        local_grad(k, c2)
        local_low(k, c2)
        one_forward(k, c1)
    for k in both:
        local_grad(k, c3)
        local_low(k, c3)
        low_start(k)
        one_start(k, c2)
    for k in both:
        one_finish(k, c0)
        two_start(k)
    for k in both:
        low_forward(k)
    for k in both:
        one_forward(k, c2)
    for k in both:
        low_second(k)
    for k in both:
        one_start(k, c3)
    for k in both:
        one_finish(k, c1)
        two_plus(k)
    for k in both:
        low_third(k)
        one_forward(k, c3)
    for k in both:
        one_finish(k, c2)
        two_minus(k)
    for k in both:
        one_finish(k, c3)
    mom1_in.wait()
    mom2_in.wait()
    wts_in.wait()
    for k in both:
        moments(k)
    tp_mark, tot_mark, last_mark = (copies.landing() for _ in range(3))
    for i, peer in enumerate(tp_peers):
        copies.send(tp_own, tp_in.at[i], peer, tp_mark)
    tot_own[6:8, :] = jnp.zeros((2, 128), F32)
    for k in both:
        resid = two_finish(k).T - own_f[k]
        own_f[k] = resid
        parts = (own_p[k] * own_p[k], own_p[k] * resid, resid * resid)
        for i, part in enumerate(parts):
            tot_own[3 * k + i : 3 * k + i + 1, :] = folded(part).sum(axis=0, keepdims=True)
    for i, peer in enumerate(fs_peers):
        copies.send(tot_own, tot_in.at[i], peer, tot_mark)
    copies.wait(tp_mark, tp_in)
    sums = tp_own[...]
    for i in range(len(tp_peers)):
        sums = sums + tp_in[i]
    ratios = [
        jnp.sqrt(jnp.sum(sums[k], keepdims=True)) / jnp.sqrt(jnp.sum(sums[2 + k], keepdims=True) + 1e-06)
        for k in both
    ]
    for k in both:
        out_u[k] = own_p[k] + ratios[k] * own_f[k]
    copies.wait(tot_mark, tot_in)
    parts = tot_own[...]
    for i in range(len(fs_peers)):
        parts = parts + tot_in[i]
    last_own[...] = parts
    for i, peer in enumerate(tp_peers):
        copies.send(last_own, last_in.at[i], peer, last_mark)
    copies.wait(last_mark, last_in)
    for i in range(len(tp_peers)):
        parts = parts + last_in[i]
    total = None
    for k in both:
        square = parts[3 * k : 3 * k + 1]
        square = square + ratios[k] * (2.0 * parts[3 * k + 1 : 3 * k + 2] + ratios[k] * parts[3 * k + 2 : 3 * k + 3])
        total = square if total is None else total + square
    scale = lax.rsqrt(jnp.sum(total, keepdims=True) / (2.0 * 2048 * 2048) + 1e-06)

    for k in range(2):
        value = out_u[k] * scale
        out_u[k] = value
        value = wts[k] - 0.02 * value
        out_w[k] = value
        gathered[k, 0, 0] = value.astype(BF16)

    upper, lower = pl.ds(0, 64), pl.ds(64, 64)

    def spread(k, b):
        marks = pending["w", k, b] = [copies.landing() for _ in range(3)]
        copies.send(gathered.at[k, 0, b], gathered.at[k, 3, b], near(axes[k][1], 1), marks[0])
        copies.send(gathered.at[k, 0, b], gathered.at[k, 1, b], near(axes[k][1], 3), marks[1])

    def relay(k, b):
        marks = pending["w", k, b]
        copies.wait(marks[0], gathered.at[k, 3, b])
        copies.send(gathered.at[k, 3, b, upper], gathered.at[k, 2, b, upper], near(axes[k][1], 1), marks[2])
        copies.wait(marks[1], gathered.at[k, 1, b])
        copies.send(gathered.at[k, 1, b, lower], gathered.at[k, 2, b, lower], near(axes[k][1], 3), marks[2])

    def land(k, b):
        copies.wait(pending["w", k, b][2], gathered.at[k, 2, b])

    def v_start(k):
        marks = pending["v", k] = [copies.landing() for _ in range(3)]
        copies.send(gathered.at[k, 0, 0], gathered.at[k, 0, 3], near(axes[k][0], 1), marks[0])
        copies.send(gathered.at[k, 0, 0], gathered.at[k, 0, 1], near(axes[k][0], 3), marks[1])

    def v_forward(k):
        marks = pending["v", k]
        copies.wait(marks[0], gathered.at[k, 0, 3])
        copies.send(gathered.at[k, 0, 3, upper], gathered.at[k, 0, 2, upper], near(axes[k][0], 1), marks[2])
        copies.wait(marks[1], gathered.at[k, 0, 1])
        copies.send(gathered.at[k, 0, 1, lower], gathered.at[k, 0, 2, lower], near(axes[k][0], 3), marks[2])

    def v_finish(k):
        copies.wait(pending["v", k][2], gathered.at[k, 0, 2])

    for k in both:
        v_start(k)
    for k in both:
        spread(k, 0)
    for k in both:
        v_forward(k)
        spread(k, 3)
        spread(k, 1)
    for k in both:
        relay(k, 0)
    for k in both:
        v_finish(k)
        spread(k, 2)
    for b in (3, 1, 2):
        for k in both:
            relay(k, b)
    for b in (0, 3, 1, 2):
        for k in both:
            land(k, b)
    copies.wait_sent()


def write_out(
    out_w, out_u, out_1, out_2, gathered, new_weights, update, new_first, new_second, weight_copy, sems
):
    z, x = lax.axis_index(Z), lax.axis_index(X)
    pairs = []
    for a in range(4):
        for b in range(4):
            for k in range(2):
                dz, dx = (a, b) if k == 0 else (b, a)
                block = lax.rem(z + dz, 4) * 4 + lax.rem(x + dx, 4)
                rows = pl.ds(pl.multiple_of(block * 128, 128), 128)
                pairs.append((gathered.at[k, a, b], weight_copy.at[k, rows, :]))
    for src, dst in pairs:
        pltpu.make_async_copy(src, dst, sems.at[0]).start()
    pairs = ((out_1, new_first), (out_2, new_second), (out_w, new_weights), (out_u, update))
    copies = [pltpu.make_async_copy(*pair, sems.at[1 + i]) for i, pair in enumerate(pairs)]
    for copy in copies:
        copy.start()
    for copy in copies:
        copy.wait()
    pltpu.make_async_copy(gathered, gathered, sems.at[0]).wait()


def per_device(*args):
    any_space = pl.BlockSpec(memory_space=pl.ANY)
    vmem_space = pl.BlockSpec(memory_space=pltpu.VMEM)
    held = (
        ((2, 128, 256), F32),
        ((2, 128, 256), F32),
        ((2, 256, 256), F32),
        ((2, 256, 256), F32),
        ((2, 4, 4, 128, 256), BF16),
    )
    dma = pltpu.SemaphoreType.DMA
    results = pl.pallas_call(
        kernel,
        name="step",
        out_shape=[pltpu.VMEM(*shape) for shape in held],
        in_specs=[any_space] * 8,
        out_specs=[vmem_space] * 5,
        scratch_shapes=[
            pltpu.VMEM((2, 4, 2560, 512), BF16),
            pltpu.VMEM((2, 2560, 256), BF16),
            pltpu.VMEM((2, 256, 2560), BF16),
            pltpu.VMEM((2, 4, 512, 256), BF16),
            pltpu.VMEM((2, 4, 4, 256, 128), F32),
            pltpu.VMEM((2, 4, 2, 128, 128), F32),
            pltpu.VMEM((2, 4, 2, 2, 128, 128), F32),
            pltpu.VMEM((2, 2, 128, 128), F32),
            pltpu.VMEM((2, 2, 2, 128, 128), F32),
            pltpu.VMEM((2, 256, 256), F32),
            pltpu.VMEM((2, 2, 32, 256), F32),
            pltpu.VMEM((2, 2, 2, 32, 256), F32),
            pltpu.VMEM((2, 3, 16, 256), F32),
            pltpu.VMEM((2, 256, 256), F32),
            pltpu.VMEM((2, 128, 256), F32),
            pltpu.VMEM((2, 256, 256), F32),
            pltpu.VMEM((2, 256, 256), F32),
            pltpu.VMEM((2, 128, 256), F32),
            pltpu.VMEM((2, 128, 256), F32),
            pltpu.VMEM((4, 8, 128), F32),
            pltpu.VMEM((7, 4, 8, 128), F32),
            pltpu.VMEM((8, 128), F32),
            pltpu.VMEM((15, 8, 128), F32),
            pltpu.VMEM((8, 128), F32),
            pltpu.VMEM((7, 8, 128), F32),
            dma((LOADS,)),
            dma((SENDS,)),
            dma((LANDINGS,)),
        ],
        compiler_params=pltpu.CompilerParams(
            collective_id=0, has_side_effects=True, vmem_limit_bytes=60 * 1024 * 1024
        ),
    )(*args)
    return pl.pallas_call(
        write_out,
        name="write_out",
        out_shape=[jax.ShapeDtypeStruct(shape, kind) for shape, kind in held[:4]]
        + [jax.ShapeDtypeStruct((2, 2048, 256), BF16)],
        in_specs=[vmem_space] * 5,
        out_specs=[any_space] * 5,
        scratch_shapes=[dma((5,))],
        compiler_params=pltpu.CompilerParams(vmem_limit_bytes=1024 * 1024),
    )(*results)


def solution(mesh):
    finer = Mesh(mesh.devices.reshape(4, 4, 4, 2), (Z, X, Y, C))
    in_specs = (
        P(FS, None),
        P(FS, None),
        P(FS, TP),
        P(FS, TP),
        P(None, FS, TP),
        P(),
        P(None, None, TP),
        P(None, None, TP),
    )
    out_specs = (
        P(None, FS, TP),
        P(None, FS, TP),
        P(None, None, TP),
        P(None, None, TP),
        P(None, None, TP),
    )
    return jax.shard_map(per_device, mesh=finer, in_specs=in_specs, out_specs=out_specs, check_vma=False)
```

time: 81.3 us -> 73.3 us (0.902)
  Pallas kernels: 80.6 us -> 72.6 us
    pallas_call x1, Pallas kernels: 78.4 us -> 70.7 us  [per_device(): pl.pallas_call(kernel, name='step', out_shape=[pltpu.VMEM(*shape) for sha...]
where the time goes in v3:
time: 73.3 us; the launch traced here: 73.2 us
  Pallas kernels  72.6 us (99%)
    pallas_call x1, Pallas kernels, per_device(): pl.pallas_call(kernel, name='step', out_shape=[pltpu.VMEM(*shape) for sha...  70.7 us
    pallas_call x1, Pallas kernels, per_device(): pl.pallas_call(write_out, name='write_out', out_shape=[jax.ShapeDtypeStru...  1.87 us

profile of v3, /device:TPU:0, one launch (start us, length us, event | category | flops | bytes accessed | tf_op | source)
XLA Modules:
  0.0 73.2 jit_solution(4739745215250303950)
XLA Ops:
  0.6 70.7 %step.1 = (f32[2,128,256]{2,1,0:T(8,128)S(1)}, f32[2,128,256]{2,1,0:T(8,128)S(1)}, f32[2,256,256]{2,1,0:T(8,128)S(1)}, f32[2,256,256]{2,1,0:T(8,128)S(1)}, bf16[2,4,4,128,256]{4,3,2,1,0:T(8,128)(2,1)S(1)}) custom-call(bf16[2560,2048]{1,0:T(8,128)(2,1)} %layer_inputs.1, bf16[2560,2048]{1,0:T(8,128)(2,1)} %output_cot.1, bf16[2560,256]{1,0:T(8,128)(2,1)} %query_cot.1, ...), custom_call_target="tpu_custom_call" | custom-call | tf_op jit(solution)/shard_map/step/pallas_call | solution.py:462
  71.4 1.9 %write_out.1 = (f32[2,128,256]{2,1,0:T(8,128)}, f32[2,128,256]{2,1,0:T(8,128)}, f32[2,256,256]{2,1,0:T(8,128)}, f32[2,256,256]{2,1,0:T(8,128)}, bf16[2,2048,256]{2,1,0:T(8,128)(2,1)}) custom-call(f32[2,128,256]{2,1,0:T(8,128)S(1)} %get-tuple-element.10.out_w, f32[2,128,256]{2,1,0:T(8,128)S(1)} %get-tuple-element.11.out_u, ...), custom_call_target="tpu_custom_call" | custom-call | tf_op jit(solution)/shard_map/write_out/pallas_call | solution.py:502

commit v4 on v3

--- a/solution.py
+++ b/solution.py
@@ -24,15 +24,16 @@
         self.landings += 1
         return self.landings - 1
 
-    def send(self, src, dst, device, landing):
+    def send(self, src, dst, device, landing, own=None):
         size = math.prod(src.shape) * src.dtype.itemsize // 1024
-        if self.sent[-1] + size > self.spare.shape[0]:
-            self.sent.append(0)
-        self.sent[-1] += size
+        if own is None:
+            if self.sent[-1] + size > self.spare.shape[0]:
+                self.sent.append(0)
+            self.sent[-1] += size
         pltpu.make_async_remote_copy(
             src_ref=src,
             dst_ref=dst,
-            send_sem=self.send_sems.at[len(self.sent) - 1],
+            send_sem=self.send_sems.at[len(self.sent) - 1 if own is None else own],
             recv_sem=self.recv_sems.at[landing],
             device_id=device,
             device_id_type=MESH,
@@ -47,7 +48,7 @@
             pltpu.make_async_copy(rows, rows, self.send_sems.at[index]).wait()
 
 
-SENDS, LANDINGS, LOADS = 3, 73, 15
+SENDS, LANDINGS, LOADS = 4, 72, 15
 
 
 def halves(value, terms):
@@ -73,7 +74,7 @@
     out_w, out_u, out_1, out_2, gathered,
     left, right, right_t, fact, grad, one_a, one_b, two_a, two_b,
     low_t, low_a, low_b, low_in, low_all, wts, mom1, mom2,
-    own_p, own_f, tp_own, tp_in, tot_own, tot_in, last_own, last_in,
+    own_p, own_f, tp_own, tp_in, tot_own, tot_in,
     load_sems, send_sems, recv_sems,
 ):
     z, x, y, c = (lax.axis_index(name) for name in (Z, X, Y, C))
@@ -135,6 +136,14 @@
     tp_peers = [
         {Y: lax.rem(y + dy, 4), C: lax.rem(c + dc, 2)} for dy in range(4) for dc in range(2) if dy or dc
     ]
+    all_peers = [
+        {Z: lax.rem(z + dz, 4), X: lax.rem(x + dx, 4), Y: lax.rem(y + dy, 4), C: lax.rem(c + dc, 2)}
+        for dz in ORDER
+        for dx in ORDER
+        for dy in ORDER
+        for dc in range(2)
+        if dz or dx or dy or dc
+    ]
     for peer in fs_peers + tp_peers:
         pl.semaphore_signal(barrier, inc=1, device_id=peer, device_id_type=MESH)
 
@@ -303,18 +312,18 @@
         two_start(k)
     for k in both:
         low_forward(k)
+        one_start(k, c3)
     for k in both:
         one_forward(k, c2)
     for k in both:
         low_second(k)
-    for k in both:
-        one_start(k, c3)
     for k in both:
         one_finish(k, c1)
         two_plus(k)
     for k in both:
+        one_forward(k, c3)
+    for k in both:
         low_third(k)
-        one_forward(k, c3)
     for k in both:
         one_finish(k, c2)
         two_minus(k)
@@ -325,44 +334,34 @@
     wts_in.wait()
     for k in both:
         moments(k)
-    tp_mark, tot_mark, last_mark = (copies.landing() for _ in range(3))
+    tp_mark, tot_mark = copies.landing(), copies.landing()
     for i, peer in enumerate(tp_peers):
         copies.send(tp_own, tp_in.at[i], peer, tp_mark)
-    tot_own[6:8, :] = jnp.zeros((2, 128), F32)
+    lane = lax.broadcasted_iota(jnp.int32, (1, 128), 1)
+    row = jnp.zeros((1, 128), F32)
     for k in both:
         resid = two_finish(k).T - own_f[k]
         own_f[k] = resid
         parts = (own_p[k] * own_p[k], own_p[k] * resid, resid * resid)
         for i, part in enumerate(parts):
-            tot_own[3 * k + i : 3 * k + i + 1, :] = folded(part).sum(axis=0, keepdims=True)
-    for i, peer in enumerate(fs_peers):
-        copies.send(tot_own, tot_in.at[i], peer, tot_mark)
+            row = jnp.where(lane == 3 * k + i, jnp.sum(folded(part), keepdims=True), row)
+    tot_own[0:1, :] = row
+    tot_in[127:128, :] = row
+    for i, peer in enumerate(all_peers):
+        copies.send(tot_own.at[pl.ds(0, 1)], tot_in.at[pl.ds(i, 1)], peer, tot_mark, SENDS - 1)
     copies.wait(tp_mark, tp_in)
     sums = tp_own[...]
     for i in range(len(tp_peers)):
         sums = sums + tp_in[i]
-    ratios = [
-        jnp.sqrt(jnp.sum(sums[k], keepdims=True)) / jnp.sqrt(jnp.sum(sums[2 + k], keepdims=True) + 1e-06)
-        for k in both
-    ]
-    for k in both:
-        out_u[k] = own_p[k] + ratios[k] * own_f[k]
-    copies.wait(tot_mark, tot_in)
-    parts = tot_own[...]
-    for i in range(len(fs_peers)):
-        parts = parts + tot_in[i]
-    last_own[...] = parts
-    for i, peer in enumerate(tp_peers):
-        copies.send(last_own, last_in.at[i], peer, last_mark)
-    copies.wait(last_mark, last_in)
-    for i in range(len(tp_peers)):
-        parts = parts + last_in[i]
-    total = None
-    for k in both:
-        square = parts[3 * k : 3 * k + 1]
-        square = square + ratios[k] * (2.0 * parts[3 * k + 1 : 3 * k + 2] + ratios[k] * parts[3 * k + 2 : 3 * k + 3])
-        total = square if total is None else total + square
-    scale = lax.rsqrt(jnp.sum(total, keepdims=True) / (2.0 * 2048 * 2048) + 1e-06)
+    factor = jnp.zeros((1, 128), F32)
+    for k in both:
+        ratio = jnp.sqrt(jnp.sum(sums[k], keepdims=True)) / jnp.sqrt(jnp.sum(sums[2 + k], keepdims=True) + 1e-06)
+        out_u[k] = own_p[k] + ratio * own_f[k]
+        for i, value in enumerate((jnp.ones((1, 1), F32), 2.0 * ratio, ratio * ratio)):
+            factor = jnp.where(lane == 3 * k + i, value, factor)
+    copies.wait(tot_mark, tot_in.at[pl.ds(0, 127)])
+    total = jnp.sum(folded(tot_in[...]).sum(axis=0, keepdims=True) * factor, keepdims=True)
+    scale = lax.rsqrt(total / (2.0 * 2048 * 2048) + 1e-06)
 
     for k in range(2):
         value = out_u[k] * scale
@@ -423,6 +422,7 @@
         for k in both:
             land(k, b)
     copies.wait_sent()
+    pltpu.make_async_copy(tot_in.at[pl.ds(0, 127)], tot_in.at[pl.ds(0, 127)], send_sems.at[SENDS - 1]).wait()
 
 
 def write_out(
@@ -488,9 +488,7 @@
             pltpu.VMEM((4, 8, 128), F32),
             pltpu.VMEM((7, 4, 8, 128), F32),
             pltpu.VMEM((8, 128), F32),
-            pltpu.VMEM((15, 8, 128), F32),
-            pltpu.VMEM((8, 128), F32),
-            pltpu.VMEM((7, 8, 128), F32),
+            pltpu.VMEM((128, 128), F32),
             dma((LOADS,)),
             dma((SENDS,)),
             dma((LANDINGS,)),

time: 73.3 us -> 70.8 us (0.966)
  Pallas kernels: 72.6 us -> 70.1 us
    pallas_call x1, Pallas kernels: 70.7 us -> 68.2 us  [per_device(): pl.pallas_call(kernel, name='step', out_shape=[pltpu.VMEM(*shape) for sha...]
where the time goes in v4:
time: 70.8 us; the launch traced here: 70.7 us
  Pallas kernels  70.1 us (99%)
    pallas_call x1, Pallas kernels, per_device(): pl.pallas_call(kernel, name='step', out_shape=[pltpu.VMEM(*shape) for sha...  68.2 us
    pallas_call x1, Pallas kernels, per_device(): pl.pallas_call(write_out, name='write_out', out_shape=[jax.ShapeDtypeStru...  1.87 us

profile of v4, /device:TPU:0, one launch (start us, length us, event | category | flops | bytes accessed | tf_op | source)
XLA Modules:
  0.0 70.7 jit_solution(17287331356716772482)
XLA Ops:
  0.6 68.2 %step.1 = (f32[2,128,256]{2,1,0:T(8,128)S(1)}, f32[2,128,256]{2,1,0:T(8,128)S(1)}, f32[2,256,256]{2,1,0:T(8,128)S(1)}, f32[2,256,256]{2,1,0:T(8,128)S(1)}, bf16[2,4,4,128,256]{4,3,2,1,0:T(8,128)(2,1)S(1)}) custom-call(bf16[2560,2048]{1,0:T(8,128)(2,1)} %layer_inputs.1, bf16[2560,2048]{1,0:T(8,128)(2,1)} %output_cot.1, bf16[2560,256]{1,0:T(8,128)(2,1)} %query_cot.1, ...), custom_call_target="tpu_custom_call" | custom-call | tf_op jit(solution)/shard_map/step/pallas_call | solution.py:462
  68.8 1.9 %write_out.1 = (f32[2,128,256]{2,1,0:T(8,128)}, f32[2,128,256]{2,1,0:T(8,128)}, f32[2,256,256]{2,1,0:T(8,128)}, f32[2,256,256]{2,1,0:T(8,128)}, bf16[2,2048,256]{2,1,0:T(8,128)(2,1)}) custom-call(f32[2,128,256]{2,1,0:T(8,128)S(1)} %get-tuple-element.10.out_w, f32[2,128,256]{2,1,0:T(8,128)S(1)} %get-tuple-element.11.out_u, ...), custom_call_target="tpu_custom_call" | custom-call | tf_op jit(solution)/shard_map/write_out/pallas_call | solution.py:500

commit v5 on v4

--- a/solution.py
+++ b/solution.py
@@ -48,7 +48,7 @@
             pltpu.make_async_copy(rows, rows, self.send_sems.at[index]).wait()
 
 
-SENDS, LANDINGS, LOADS = 4, 72, 15
+SENDS, LANDINGS, LOADS = 4, 77, 15
 
 
 def halves(value, terms):
@@ -74,7 +74,7 @@
     out_w, out_u, out_1, out_2, gathered,
     left, right, right_t, fact, grad, one_a, one_b, two_a, two_b,
     low_t, low_a, low_b, low_in, low_all, wts, mom1, mom2,
-    own_p, own_f, tp_own, tp_in, tot_own, tot_in,
+    own_p, own_f, own_g, grams, mom1_t, mom2_t, tot_own, tot_in,
     load_sems, send_sems, recv_sems,
 ):
     z, x, y, c = (lax.axis_index(name) for name in (Z, X, Y, C))
@@ -264,23 +264,67 @@
         rows = low_piece(k, 0)
         low_all[k, rows] = low_t[k, rows] + low_in[k, 0] + low_in[k, 1] + low_in[k, 2]
         mark = pending["low3", k] = copies.landing()
-        for peer in fs_peers:
-            copies.send(low_all.at[k, rows], low_all.at[k, rows], peer, mark)
+        for a in (2, 1, 3):
+            copies.send(low_all.at[k, rows], low_all.at[k, rows], near(axes[k][1], a), mark)
+
+    def low_fourth(k):
+        copies.wait(pending["low3", k], low_all.at[k, pl.ds(0, 48)])
+        axis, rows = axes[k][0], low_rows(k, 0)
+        marks = pending["low4", k] = [copies.landing() for _ in range(3)]
+        copies.send(low_all.at[k, rows], low_all.at[k, rows], near(axis, 1), marks[0])
+        copies.send(low_all.at[k, rows], low_all.at[k, rows], near(axis, 3), marks[1])
+
+    def low_fifth(k):
+        axis, marks = axes[k][0], pending["low4", k]
+        copies.wait(marks[0], low_all.at[k, pl.ds(0, 64)])
+        rows = low_rows(k, 3, 0)
+        copies.send(low_all.at[k, rows], low_all.at[k, rows], near(axis, 1), marks[2])
+        copies.wait(marks[1], low_all.at[k, pl.ds(0, 64)])
+        rows = low_rows(k, 1, 1)
+        copies.send(low_all.at[k, rows], low_all.at[k, rows], near(axis, 3), marks[2])
+
+    def gram(k):
+        total = None
+        for a in range(4):
+            rows = fact[k, a]
+            term = jnp.dot(rows.T, rows, preferred_element_type=F32)
+            total = term if total is None else total + term
+        for i, part in enumerate(halves(total, 2)):
+            grams[k, i] = part
+
+    def turn(k):
+        mom1_t[k] = mom1[k].T
+        mom2_t[k] = mom2[k].T
+
+    def own_terms(k):
+        rows = low_piece(k, 0)
+        low = low_all[k, rows, :]
+        first = 0.9 * mom1_t[k, rows, :] + 0.1 * low
+        second = 0.95 * mom2_t[k, rows, :] + 0.05 * low * low
+        normed = first / (jnp.sqrt(second) + 1e-06)
+        stack = jnp.concatenate(halves(normed, 2) + halves(low, 2), axis=0)
+        product = sum(jnp.dot(stack, grams[k, i], preferred_element_type=F32) for i in range(2))
+        by_normed = product[0:16] + product[16:32]
+        by_low = product[32:48] + product[48:64]
+        pairs = ((normed, by_normed), (normed, low), (normed, by_low), (low, low), (low, by_low), (normed, normed))
+        row = jnp.zeros((1, 128), F32)
+        for i, (one, other) in enumerate(pairs):
+            row = jnp.where(lane == 8 * k + i, jnp.sum(folded(one * other), keepdims=True), row)
+        return row
 
     def moments(k):
-        copies.wait(pending["low3", k], low_all.at[k, pl.ds(0, 240)])
+        copies.wait(pending["low4", k][2], low_all.at[k, pl.ds(0, 64)])
         low = low_all[k].T
         first = 0.9 * mom1[k] + 0.1 * low
         second = 0.95 * mom2[k] + 0.05 * low * low
         out_1[k] = first
         out_2[k] = second
         normed = first / (jnp.sqrt(second) + 1e-06)
-        tp_own[k] = folded(normed * normed)
-        tp_own[2 + k] = folded(low * low)
         mine = fact[k, 0, 0:128, :]
         own_p[k] = sum(jnp.dot(mine, part, preferred_element_type=F32) for part in halves(normed, 3))
-        own_f[k] = sum(jnp.dot(mine, part, preferred_element_type=F32) for part in halves(low, 3))
-
+        own_f[k] = own_g[k].T - sum(jnp.dot(mine, part, preferred_element_type=F32) for part in halves(low, 3))
+
+    lane = lax.broadcasted_iota(jnp.int32, (1, 128), 1)
     both = range(2)
     c0, c1, c2, c3 = ORDER
     for k in both:
@@ -311,60 +355,60 @@
         one_finish(k, c0)
         two_start(k)
     for k in both:
+        gram(k)
+    for k in both:
         low_forward(k)
         one_start(k, c3)
     for k in both:
         one_forward(k, c2)
-    for k in both:
-        low_second(k)
-    for k in both:
-        one_finish(k, c1)
-        two_plus(k)
-    for k in both:
-        one_forward(k, c3)
-    for k in both:
-        low_third(k)
-    for k in both:
-        one_finish(k, c2)
-        two_minus(k)
-    for k in both:
-        one_finish(k, c3)
     mom1_in.wait()
     mom2_in.wait()
     wts_in.wait()
     for k in both:
-        moments(k)
-    tp_mark, tot_mark = copies.landing(), copies.landing()
-    for i, peer in enumerate(tp_peers):
-        copies.send(tp_own, tp_in.at[i], peer, tp_mark)
-    lane = lax.broadcasted_iota(jnp.int32, (1, 128), 1)
-    row = jnp.zeros((1, 128), F32)
-    for k in both:
-        resid = two_finish(k).T - own_f[k]
-        own_f[k] = resid
-        parts = (own_p[k] * own_p[k], own_p[k] * resid, resid * resid)
-        for i, part in enumerate(parts):
-            row = jnp.where(lane == 3 * k + i, jnp.sum(folded(part), keepdims=True), row)
+        turn(k)
+    for k in both:
+        low_second(k)
+    for k in both:
+        one_finish(k, c1)
+        two_plus(k)
+    for k in both:
+        one_forward(k, c3)
+    for k in both:
+        low_third(k)
+    for k in both:
+        one_finish(k, c2)
+        two_minus(k)
+    row = own_terms(0) + own_terms(1)
+    for k in both:
+        one_finish(k, c3)
+    for k in both:
+        own = two_finish(k)
+        own_g[k] = own
+        row = jnp.where(lane == 8 * k + 6, jnp.sum(folded(own * own), keepdims=True), row)
     tot_own[0:1, :] = row
     tot_in[127:128, :] = row
+    tot_mark = copies.landing()
     for i, peer in enumerate(all_peers):
         copies.send(tot_own.at[pl.ds(0, 1)], tot_in.at[pl.ds(i, 1)], peer, tot_mark, SENDS - 1)
-    copies.wait(tp_mark, tp_in)
-    sums = tp_own[...]
-    for i in range(len(tp_peers)):
-        sums = sums + tp_in[i]
-    factor = jnp.zeros((1, 128), F32)
-    for k in both:
-        ratio = jnp.sqrt(jnp.sum(sums[k], keepdims=True)) / jnp.sqrt(jnp.sum(sums[2 + k], keepdims=True) + 1e-06)
-        out_u[k] = own_p[k] + ratio * own_f[k]
-        for i, value in enumerate((jnp.ones((1, 1), F32), 2.0 * ratio, ratio * ratio)):
-            factor = jnp.where(lane == 3 * k + i, value, factor)
+    for k in both:
+        low_fourth(k)
+    for k in both:
+        low_fifth(k)
+    for k in both:
+        moments(k)
     copies.wait(tot_mark, tot_in.at[pl.ds(0, 127)])
-    total = jnp.sum(folded(tot_in[...]).sum(axis=0, keepdims=True) * factor, keepdims=True)
-    scale = lax.rsqrt(total / (2.0 * 2048 * 2048) + 1e-06)
+    sums = folded(tot_in[...]).sum(axis=0, keepdims=True)
+    total, ratios = None, []
+    for k in both:
+        part = [jnp.sum(jnp.where(lane == 8 * k + i, sums, 0.0), keepdims=True) for i in range(7)]
+        ratio = jnp.sqrt(part[5]) / jnp.sqrt(part[3] + 1e-06)
+        value = part[0] + 2.0 * ratio * (part[1] - part[2]) + ratio * ratio * (part[6] - 2.0 * part[3] + part[4])
+        total = value if total is None else total + value
+        ratios.append(ratio)
+    scale = lax.rsqrt(jnp.maximum(total, 0.0) / (2.0 * 2048 * 2048) + 1e-06)
 
     for k in range(2):
-        value = out_u[k] * scale
+        value = (own_p[k] + ratios[k] * own_f[k]) * scale
         out_u[k] = value
         value = wts[k] - 0.02 * value
         out_w[k] = value
@@ -485,8 +529,10 @@
             pltpu.VMEM((2, 256, 256), F32),
             pltpu.VMEM((2, 128, 256), F32),
             pltpu.VMEM((2, 128, 256), F32),
-            pltpu.VMEM((4, 8, 128), F32),
-            pltpu.VMEM((7, 4, 8, 128), F32),
+            pltpu.VMEM((2, 256, 128), F32),
+            pltpu.VMEM((2, 2, 256, 256), BF16),
+            pltpu.VMEM((2, 256, 256), F32),
+            pltpu.VMEM((2, 256, 256), F32),
             pltpu.VMEM((8, 128), F32),
             pltpu.VMEM((128, 128), F32),
             dma((LOADS,)),

time: 70.8 us -> 70.5 us (level)
  no operation moved by 1% of the time
where the time goes in v5:
time: 70.5 us; the launch traced here: 70.3 us
  Pallas kernels  69.7 us (99%)
    pallas_call x1, Pallas kernels, per_device(): pl.pallas_call(kernel, name='step', out_shape=[pltpu.VMEM(*shape) for sha...  67.8 us
    pallas_call x1, Pallas kernels, per_device(): pl.pallas_call(write_out, name='write_out', out_shape=[jax.ShapeDtypeStru...  1.87 us

profile of v5, /device:TPU:0, one launch (start us, length us, event | category | flops | bytes accessed | tf_op | source)
XLA Modules:
  0.0 70.3 jit_solution(5359820782266254795)
XLA Ops:
  0.6 67.8 %step.1 = (f32[2,128,256]{2,1,0:T(8,128)S(1)}, f32[2,128,256]{2,1,0:T(8,128)S(1)}, f32[2,256,256]{2,1,0:T(8,128)S(1)}, f32[2,256,256]{2,1,0:T(8,128)S(1)}, bf16[2,4,4,128,256]{4,3,2,1,0:T(8,128)(2,1)S(1)}) custom-call(bf16[2560,2048]{1,0:T(8,128)(2,1)} %layer_inputs.1, bf16[2560,2048]{1,0:T(8,128)(2,1)} %output_cot.1, bf16[2560,256]{1,0:T(8,128)(2,1)} %query_cot.1, ...), custom_call_target="tpu_custom_call" | custom-call | tf_op jit(solution)/shard_map/step/pallas_call | solution.py:506
  68.5 1.9 %write_out.1 = (f32[2,128,256]{2,1,0:T(8,128)}, f32[2,128,256]{2,1,0:T(8,128)}, f32[2,256,256]{2,1,0:T(8,128)}, f32[2,256,256]{2,1,0:T(8,128)}, bf16[2,2048,256]{2,1,0:T(8,128)(2,1)}) custom-call(f32[2,128,256]{2,1,0:T(8,128)S(1)} %get-tuple-element.10.out_w, f32[2,128,256]{2,1,0:T(8,128)S(1)} %get-tuple-element.11.out_u, ...), custom_call_target="tpu_custom_call" | custom-call | tf_op jit(solution)/shard_map/write_out/pallas_call | solution.py:546

commit v6 on v5

--- a/solution.py
+++ b/solution.py
@@ -48,7 +48,7 @@
             pltpu.make_async_copy(rows, rows, self.send_sems.at[index]).wait()
 
 
-SENDS, LANDINGS, LOADS = 4, 77, 15
+SENDS, LANDINGS, LOADS = 4, 78, 15
 
 
 def halves(value, terms):
@@ -74,7 +74,7 @@
     out_w, out_u, out_1, out_2, gathered,
     left, right, right_t, fact, grad, one_a, one_b, two_a, two_b,
     low_t, low_a, low_b, low_in, low_all, wts, mom1, mom2,
-    own_p, own_f, own_g, grams, mom1_t, mom2_t, tot_own, tot_in,
+    own_p, own_f, own_g, grams, mom1_t, mom2_t, pair_own, pair_in, tot_own, tot_in,
     load_sems, send_sems, recv_sems,
 ):
     z, x, y, c = (lax.axis_index(name) for name in (Z, X, Y, C))
@@ -137,12 +137,11 @@
         {Y: lax.rem(y + dy, 4), C: lax.rem(c + dc, 2)} for dy in range(4) for dc in range(2) if dy or dc
     ]
     all_peers = [
-        {Z: lax.rem(z + dz, 4), X: lax.rem(x + dx, 4), Y: lax.rem(y + dy, 4), C: lax.rem(c + dc, 2)}
+        {Z: lax.rem(z + dz, 4), X: lax.rem(x + dx, 4), Y: lax.rem(y + dy, 4)}
         for dz in ORDER
         for dx in ORDER
         for dy in ORDER
-        for dc in range(2)
-        if dz or dx or dy or dc
+        if dz or dx or dy
     ]
     for peer in fs_peers + tp_peers:
         pl.semaphore_signal(barrier, inc=1, device_id=peer, device_id_type=MESH)
@@ -385,18 +384,23 @@
         own = two_finish(k)
         own_g[k] = own
         row = jnp.where(lane == 8 * k + 6, jnp.sum(folded(own * own), keepdims=True), row)
+    pair_own[0:1, :] = row
+    pair_mark, tot_mark = copies.landing(), copies.landing()
+    first_row = pl.ds(0, 1)
+    copies.send(pair_own.at[first_row], pair_in.at[first_row], {C: lax.rem(c + 1, 2)}, pair_mark, SENDS - 1)
+    copies.wait(pair_mark, pair_in.at[first_row])
+    row = row + pair_in[0:1, :]
     tot_own[0:1, :] = row
-    tot_in[127:128, :] = row
-    tot_mark = copies.landing()
+    tot_in[63:64, :] = row
     for i, peer in enumerate(all_peers):
-        copies.send(tot_own.at[pl.ds(0, 1)], tot_in.at[pl.ds(i, 1)], peer, tot_mark, SENDS - 1)
+        copies.send(tot_own.at[first_row], tot_in.at[pl.ds(i, 1)], peer, tot_mark, SENDS - 1)
     for k in both:
         low_fourth(k)
     for k in both:
         low_fifth(k)
     for k in both:
         moments(k)
-    copies.wait(tot_mark, tot_in.at[pl.ds(0, 127)])
+    copies.wait(tot_mark, tot_in.at[pl.ds(0, 63)])
     sums = folded(tot_in[...]).sum(axis=0, keepdims=True)
     total, ratios = None, []
     for k in both:
@@ -452,8 +456,9 @@
         spread(k, 0)
     for k in both:
         v_forward(k)
-        spread(k, 3)
-        spread(k, 1)
+    for b in (3, 1):
+        for k in both:
+            spread(k, b)
     for k in both:
         relay(k, 0)
     for k in both:
@@ -466,7 +471,7 @@
         for k in both:
             land(k, b)
     copies.wait_sent()
-    pltpu.make_async_copy(tot_in.at[pl.ds(0, 127)], tot_in.at[pl.ds(0, 127)], send_sems.at[SENDS - 1]).wait()
+    pltpu.make_async_copy(tot_in, tot_in, send_sems.at[SENDS - 1]).wait()
 
 
 def write_out(
@@ -534,7 +539,9 @@
             pltpu.VMEM((2, 256, 256), F32),
             pltpu.VMEM((2, 256, 256), F32),
             pltpu.VMEM((8, 128), F32),
-            pltpu.VMEM((128, 128), F32),
+            pltpu.VMEM((8, 128), F32),
+            pltpu.VMEM((8, 128), F32),
+            pltpu.VMEM((64, 128), F32),
             dma((LOADS,)),
             dma((SENDS,)),
             dma((LANDINGS,)),

time: 70.5 us -> 69 us (0.979)
  Pallas kernels: 69.7 us -> 68.2 us
    pallas_call x1, Pallas kernels: 67.8 us -> 66.4 us  [per_device(): pl.pallas_call(kernel, name='step', out_shape=[pltpu.VMEM(*shape) for sha...]
where the time goes in v6:
time: 69 us; the launch traced here: 68.9 us
  Pallas kernels  68.2 us (99%)
    pallas_call x1, Pallas kernels, per_device(): pl.pallas_call(kernel, name='step', out_shape=[pltpu.VMEM(*shape) for sha...  66.4 us
    pallas_call x1, Pallas kernels, per_device(): pl.pallas_call(write_out, name='write_out', out_shape=[jax.ShapeDtypeStru...  1.87 us

profile of v6, /device:TPU:0, one launch (start us, length us, event | category | flops | bytes accessed | tf_op | source)
XLA Modules:
  0.0 68.9 jit_solution(11971573489446984447)
XLA Ops:
  0.6 66.4 %step.1 = (f32[2,128,256]{2,1,0:T(8,128)S(1)}, f32[2,128,256]{2,1,0:T(8,128)S(1)}, f32[2,256,256]{2,1,0:T(8,128)S(1)}, f32[2,256,256]{2,1,0:T(8,128)S(1)}, bf16[2,4,4,128,256]{4,3,2,1,0:T(8,128)(2,1)S(1)}) custom-call(bf16[2560,2048]{1,0:T(8,128)(2,1)} %layer_inputs.1, bf16[2560,2048]{1,0:T(8,128)(2,1)} %output_cot.1, bf16[2560,256]{1,0:T(8,128)(2,1)} %query_cot.1, ...), custom_call_target="tpu_custom_call" | custom-call | tf_op jit(solution)/shard_map/step/pallas_call | solution.py:511
  67.0 1.9 %write_out.1 = (f32[2,128,256]{2,1,0:T(8,128)}, f32[2,128,256]{2,1,0:T(8,128)}, f32[2,256,256]{2,1,0:T(8,128)}, f32[2,256,256]{2,1,0:T(8,128)}, bf16[2,2048,256]{2,1,0:T(8,128)(2,1)}) custom-call(f32[2,128,256]{2,1,0:T(8,128)S(1)} %get-tuple-element.10.out_w, f32[2,128,256]{2,1,0:T(8,128)S(1)} %get-tuple-element.11.out_u, ...), custom_call_target="tpu_custom_call" | custom-call | tf_op jit(solution)/shard_map/write_out/pallas_call | solution.py:553

commit v7 on v6

--- a/solution.py
+++ b/solution.py
@@ -48,7 +48,7 @@
             pltpu.make_async_copy(rows, rows, self.send_sems.at[index]).wait()
 
 
-SENDS, LANDINGS, LOADS = 4, 78, 15
+SENDS, LANDINGS, LOADS = 4, 84, 15
 
 
 def halves(value, terms):
@@ -254,20 +254,17 @@
         for half in range(2):
             rows = low_rows(k, 0, half)
             low_t[k, rows] = low_t[k, rows] + (low_b[k, 0, half] + low_b[k, 1, half])
+        rows, slot = low_rows(k, 0), coord[axes[k][1]]
+        low_in[k, slot] = low_t[k, rows]
         mark = pending["low2", k] = copies.landing()
         for a in (2, 1, 3):
-            copies.send(low_t.at[k, low_piece(k, a)], low_in.at[k, 3 - a], near(axes[k][1], a), mark)
+            copies.send(low_t.at[k, rows], low_in.at[k, slot], near(axes[k][1], a), mark)
 
     def low_third(k):
-        copies.wait(pending["low2", k], low_in.at[k])
-        rows = low_piece(k, 0)
-        low_all[k, rows] = low_t[k, rows] + low_in[k, 0] + low_in[k, 1] + low_in[k, 2]
-        mark = pending["low3", k] = copies.landing()
-        for a in (2, 1, 3):
-            copies.send(low_all.at[k, rows], low_all.at[k, rows], near(axes[k][1], a), mark)
+        copies.wait(pending["low2", k], low_in.at[k, pl.ds(0, 3)])
+        low_all[k, low_rows(k, 0)] = ((low_in[k, 0] + low_in[k, 1]) + low_in[k, 2]) + low_in[k, 3]
 
     def low_fourth(k):
-        copies.wait(pending["low3", k], low_all.at[k, pl.ds(0, 48)])
         axis, rows = axes[k][0], low_rows(k, 0)
         marks = pending["low4", k] = [copies.landing() for _ in range(3)]
         copies.send(low_all.at[k, rows], low_all.at[k, rows], near(axis, 1), marks[0])
@@ -373,10 +370,11 @@
     for k in both:
         one_forward(k, c3)
     for k in both:
-        low_third(k)
-    for k in both:
         one_finish(k, c2)
         two_minus(k)
+    for k in both:
+        low_third(k)
+        low_fourth(k)
     row = own_terms(0) + own_terms(1)
     for k in both:
         one_finish(k, c3)
@@ -395,8 +393,6 @@
     for i, peer in enumerate(all_peers):
         copies.send(tot_own.at[first_row], tot_in.at[pl.ds(i, 1)], peer, tot_mark, SENDS - 1)
     for k in both:
-        low_fourth(k)
-    for k in both:
         low_fifth(k)
     for k in both:
         moments(k)
@@ -420,32 +416,49 @@
 
     upper, lower = pl.ds(0, 64), pl.ds(64, 64)
 
+    def by_halves(key, axis, block, plus, minus):
+        marks = pending[key] = [copies.landing() for _ in range(5)]
+        copies.send(block.at[upper], plus.at[upper], near(axis, 1), marks[0])
+        copies.send(block.at[lower], minus.at[lower], near(axis, 3), marks[1])
+        copies.send(block.at[lower], plus.at[lower], near(axis, 1), marks[3])
+        copies.send(block.at[upper], minus.at[upper], near(axis, 3), marks[4])
+
+    def pass_on(key, axis, plus, minus, far, whole):
+        marks = pending[key]
+        copies.wait(marks[0], plus if whole else plus.at[upper])
+        copies.send(plus.at[upper], far.at[upper], near(axis, 1), marks[2])
+        copies.wait(marks[1], minus if whole else minus.at[lower])
+        copies.send(minus.at[lower], far.at[lower], near(axis, 3), marks[2])
+
     def spread(k, b):
-        marks = pending["w", k, b] = [copies.landing() for _ in range(3)]
-        copies.send(gathered.at[k, 0, b], gathered.at[k, 3, b], near(axes[k][1], 1), marks[0])
-        copies.send(gathered.at[k, 0, b], gathered.at[k, 1, b], near(axes[k][1], 3), marks[1])
+        block, plus, minus, axis = gathered.at[k, 0, b], gathered.at[k, 3, b], gathered.at[k, 1, b], axes[k][1]
+        if b == 2:
+            by_halves(("w", k, b), axis, block, plus, minus)
+        else:
+            marks = pending["w", k, b] = [copies.landing() for _ in range(3)]
+            copies.send(block, plus, near(axis, 1), marks[0])
+            copies.send(block, minus, near(axis, 3), marks[1])
 
     def relay(k, b):
+        plus, minus, far = gathered.at[k, 3, b], gathered.at[k, 1, b], gathered.at[k, 2, b]
+        pass_on(("w", k, b), axes[k][1], plus, minus, far, b != 2)
+
+    def land(k, b):
         marks = pending["w", k, b]
-        copies.wait(marks[0], gathered.at[k, 3, b])
-        copies.send(gathered.at[k, 3, b, upper], gathered.at[k, 2, b, upper], near(axes[k][1], 1), marks[2])
-        copies.wait(marks[1], gathered.at[k, 1, b])
-        copies.send(gathered.at[k, 1, b, lower], gathered.at[k, 2, b, lower], near(axes[k][1], 3), marks[2])
-
-    def land(k, b):
-        copies.wait(pending["w", k, b][2], gathered.at[k, 2, b])
+        if b == 2:
+            copies.wait(marks[3], gathered.at[k, 3, b, lower])
+            copies.wait(marks[4], gathered.at[k, 1, b, upper])
+        copies.wait(marks[2], gathered.at[k, 2, b])
 
     def v_start(k):
-        marks = pending["v", k] = [copies.landing() for _ in range(3)]
-        copies.send(gathered.at[k, 0, 0], gathered.at[k, 0, 3], near(axes[k][0], 1), marks[0])
-        copies.send(gathered.at[k, 0, 0], gathered.at[k, 0, 1], near(axes[k][0], 3), marks[1])
+        by_halves(("v", k), axes[k][0], gathered.at[k, 0, 0], gathered.at[k, 0, 3], gathered.at[k, 0, 1])
 
     def v_forward(k):
-        marks = pending["v", k]
-        copies.wait(marks[0], gathered.at[k, 0, 3])
-        copies.send(gathered.at[k, 0, 3, upper], gathered.at[k, 0, 2, upper], near(axes[k][0], 1), marks[2])
-        copies.wait(marks[1], gathered.at[k, 0, 1])
-        copies.send(gathered.at[k, 0, 1, lower], gathered.at[k, 0, 2, lower], near(axes[k][0], 3), marks[2])
+        pass_on(("v", k), axes[k][0], gathered.at[k, 0, 3], gathered.at[k, 0, 1], gathered.at[k, 0, 2], False)
+
+    def v_rest(k):
+        copies.wait(pending["v", k][3], gathered.at[k, 0, 3, lower])
+        copies.wait(pending["v", k][4], gathered.at[k, 0, 1, upper])
 
     def v_finish(k):
         copies.wait(pending["v", k][2], gathered.at[k, 0, 2])
@@ -456,6 +469,8 @@
         spread(k, 0)
     for k in both:
         v_forward(k)
+    for k in both:
+        v_rest(k)
     for b in (3, 1):
         for k in both:
             spread(k, b)
@@ -527,7 +542,7 @@
             pltpu.VMEM((2, 256, 256), F32),
             pltpu.VMEM((2, 2, 32, 256), F32),
             pltpu.VMEM((2, 2, 2, 32, 256), F32),
-            pltpu.VMEM((2, 3, 16, 256), F32),
+            pltpu.VMEM((2, 4, 64, 256), F32),
             pltpu.VMEM((2, 256, 256), F32),
             pltpu.VMEM((2, 128, 256), F32),
             pltpu.VMEM((2, 256, 256), F32),

time: 69 us -> 65.5 us (0.949)
  Pallas kernels: 68.2 us -> 64.7 us
    pallas_call x1, Pallas kernels: 66.4 us -> 62.8 us  [per_device(): pl.pallas_call(kernel, name='step', out_shape=[pltpu.VMEM(*shape) for sha...]
where the time goes in v7:
time: 65.5 us; the launch traced here: 65.4 us
  Pallas kernels  64.7 us (99%)
    pallas_call x1, Pallas kernels, per_device(): pl.pallas_call(kernel, name='step', out_shape=[pltpu.VMEM(*shape) for sha...  62.8 us
    pallas_call x1, Pallas kernels, per_device(): pl.pallas_call(write_out, name='write_out', out_shape=[jax.ShapeDtypeStru...  1.87 us

profile of v7, /device:TPU:0, one launch (start us, length us, event | category | flops | bytes accessed | tf_op | source)
XLA Modules:
  0.0 65.4 jit_solution(1577409790909216500)
XLA Ops:
  0.6 62.8 %step.1 = (f32[2,128,256]{2,1,0:T(8,128)S(1)}, f32[2,128,256]{2,1,0:T(8,128)S(1)}, f32[2,256,256]{2,1,0:T(8,128)S(1)}, f32[2,256,256]{2,1,0:T(8,128)S(1)}, bf16[2,4,4,128,256]{4,3,2,1,0:T(8,128)(2,1)S(1)}) custom-call(bf16[2560,2048]{1,0:T(8,128)(2,1)} %layer_inputs.1, bf16[2560,2048]{1,0:T(8,128)(2,1)} %output_cot.1, bf16[2560,256]{1,0:T(8,128)(2,1)} %query_cot.1, ...), custom_call_target="tpu_custom_call" | custom-call | tf_op jit(solution)/shard_map/step/pallas_call | solution.py:526
  63.5 1.9 %write_out.1 = (f32[2,128,256]{2,1,0:T(8,128)}, f32[2,128,256]{2,1,0:T(8,128)}, f32[2,256,256]{2,1,0:T(8,128)}, f32[2,256,256]{2,1,0:T(8,128)}, bf16[2,2048,256]{2,1,0:T(8,128)(2,1)}) custom-call(f32[2,128,256]{2,1,0:T(8,128)S(1)} %get-tuple-element.10.out_w, f32[2,128,256]{2,1,0:T(8,128)S(1)} %get-tuple-element.11.out_u, ...), custom_call_target="tpu_custom_call" | custom-call | tf_op jit(solution)/shard_map/write_out/pallas_call | solution.py:568

commit v8 on v7

--- a/solution.py
+++ b/solution.py
@@ -48,7 +48,7 @@
             pltpu.make_async_copy(rows, rows, self.send_sems.at[index]).wait()
 
 
-SENDS, LANDINGS, LOADS = 4, 84, 15
+SENDS, LANDINGS, LOADS = 4, 46, 15
 
 
 def halves(value, terms):
@@ -318,7 +318,7 @@
         normed = first / (jnp.sqrt(second) + 1e-06)
         mine = fact[k, 0, 0:128, :]
         own_p[k] = sum(jnp.dot(mine, part, preferred_element_type=F32) for part in halves(normed, 3))
-        own_f[k] = own_g[k].T - sum(jnp.dot(mine, part, preferred_element_type=F32) for part in halves(low, 3))
+        own_f[k] = own_g[k] - sum(jnp.dot(mine, part, preferred_element_type=F32) for part in halves(low, 3))
 
     lane = lax.broadcasted_iota(jnp.int32, (1, 128), 1)
     both = range(2)
@@ -354,9 +354,9 @@
         gram(k)
     for k in both:
         low_forward(k)
+    for k in both:
+        one_forward(k, c2)
         one_start(k, c3)
-    for k in both:
-        one_forward(k, c2)
     mom1_in.wait()
     mom2_in.wait()
     wts_in.wait()
@@ -380,7 +380,7 @@
         one_finish(k, c3)
     for k in both:
         own = two_finish(k)
-        own_g[k] = own
+        own_g[k] = own.T
         row = jnp.where(lane == 8 * k + 6, jnp.sum(folded(own * own), keepdims=True), row)
     pair_own[0:1, :] = row
     pair_mark, tot_mark = copies.landing(), copies.landing()
@@ -463,6 +463,7 @@
     def v_finish(k):
         copies.wait(pending["v", k][2], gathered.at[k, 0, 2])
 
+    copies.landings = 0
     for k in both:
         v_start(k)
     for k in both:
@@ -549,7 +550,7 @@
             pltpu.VMEM((2, 256, 256), F32),
             pltpu.VMEM((2, 128, 256), F32),
             pltpu.VMEM((2, 128, 256), F32),
-            pltpu.VMEM((2, 256, 128), F32),
+            pltpu.VMEM((2, 128, 256), F32),
             pltpu.VMEM((2, 2, 256, 256), BF16),
             pltpu.VMEM((2, 256, 256), F32),
             pltpu.VMEM((2, 256, 256), F32),

time: 65.5 us -> 65.2 us (level)
  no operation moved by 1% of the time
where the time goes in v8:
time: 65.2 us; the launch traced here: 65.1 us
  Pallas kernels  64.4 us (99%)
    pallas_call x1, Pallas kernels, per_device(): pl.pallas_call(kernel, name='step', out_shape=[pltpu.VMEM(*shape) for sha...  62.5 us
    pallas_call x1, Pallas kernels, per_device(): pl.pallas_call(write_out, name='write_out', out_shape=[jax.ShapeDtypeStru...  1.87 us

profile of v8, /device:TPU:0, one launch (start us, length us, event | category | flops | bytes accessed | tf_op | source)
XLA Modules:
  0.0 65.1 jit_solution(11848427819418442759)
XLA Ops:
  0.6 62.5 %step.1 = (f32[2,128,256]{2,1,0:T(8,128)S(1)}, f32[2,128,256]{2,1,0:T(8,128)S(1)}, f32[2,256,256]{2,1,0:T(8,128)S(1)}, f32[2,256,256]{2,1,0:T(8,128)S(1)}, bf16[2,4,4,128,256]{4,3,2,1,0:T(8,128)(2,1)S(1)}) custom-call(bf16[2560,2048]{1,0:T(8,128)(2,1)} %layer_inputs.1, bf16[2560,2048]{1,0:T(8,128)(2,1)} %output_cot.1, bf16[2560,256]{1,0:T(8,128)(2,1)} %query_cot.1, ...), custom_call_target="tpu_custom_call" | custom-call | tf_op jit(solution)/shard_map/step/pallas_call | solution.py:527
  63.2 1.9 %write_out.1 = (f32[2,128,256]{2,1,0:T(8,128)}, f32[2,128,256]{2,1,0:T(8,128)}, f32[2,256,256]{2,1,0:T(8,128)}, f32[2,256,256]{2,1,0:T(8,128)}, bf16[2,2048,256]{2,1,0:T(8,128)(2,1)}) custom-call(f32[2,128,256]{2,1,0:T(8,128)S(1)} %get-tuple-element.10.out_w, f32[2,128,256]{2,1,0:T(8,128)S(1)} %get-tuple-element.11.out_u, ...), custom_call_target="tpu_custom_call" | custom-call | tf_op jit(solution)/shard_map/write_out/pallas_call | solution.py:569
